TPU v7x, 256 devices: a whole 4x4x8 slice. The times are simulated.
256 devices in a mesh: sp: 32 (over z, x), tp: 8 (over y, core).
Axes of the slice: x: 4, y: 4, z: 8, core: 2. Of those that a mesh axis runs over, the one named last changes fastest.
Arguments:
- inputs: bfloat16 [32768, 2048], P('sp', 'tp'), may hold values from -6 to 6
- w_query: bfloat16 [2048, 2048], P(None, 'tp'), may hold values from -0.125 to 0.125
- w_value: bfloat16 [2048, 2048], P(None, 'tp'), may hold values from -0.125 to 0.125
- w_forget: bfloat16 [2, 2048, 2048], P(None, None, 'tp'), may hold values from -0.125 to 0.125
- w_gate: bfloat16 [2048, 2048], P(None, 'tp'), may hold values from -0.125 to 0.125
- gate_room: float32 [2, 2048], P(None, 'tp'), as said below
- extra_decay: float32 [16, 32768], P('tp', 'sp'), may hold values from -2 to 0
- out_gain: float32 [2048], P('tp'), may hold values from 0.1 to 1.9
- new_inputs: bfloat16 [128, 2048], replicated, may hold values from -6 to 6
Outputs:
- mixed_rows: bfloat16 [32768, 2048], P('sp', 'tp')
- prompt_state_cache: bfloat16 [16, 128, 128], P('tp')
- new_read: bfloat16 [128, 2048], P(None, 'tp')
Inputs may be any that keep to these rules, and one draw needn't show every extreme that they name: `gate_room`: each entry lies between 0.5 / 32768 and 0.1.
All inputs are finite; a program needn't handle non-finite values.
Results may differ from a plain program's by a relative error of at most 0.012.
The roundings to bfloat16 on the way count: a program that leaves them out, or rounds other values in their place, can miss the bound.
Values may be sent and summed in bfloat16 or wider, within the bound.
A program may use at most 128 MiB of HBM per device.

v0:
```python
import jax
import jax.numpy as jnp
from jax import lax
from jax.experimental import pallas as pl
from jax.experimental.pallas import tpu as pltpu
from jax.sharding import PartitionSpec as P

MESH = pl.DeviceIdType.MESH
EPS = 1e-06
B = 128
HD = 128
F32 = jnp.float32
BF16 = jnp.bfloat16


def nn(a, b):
    return lax.dot_general(a, b, (((1,), (0,)), ((), ())), preferred_element_type=F32)


def nt(a, b):
    return lax.dot_general(a, b, (((1,), (1,)), ((), ())), preferred_element_type=F32)


def tn(a, b):
    return lax.dot_general(a, b, (((0,), (0,)), ((), ())), preferred_element_type=F32)


def split2(a):
    hi = a.astype(BF16)
    return hi, (a - hi.astype(F32)).astype(BF16)


def log_one_minus(k):
    s = jnp.full_like(k, 1.0 / 8.0)
    for n in (7, 6, 5, 4, 3, 2):
        s = s * k + (1.0 / n)
    return -(s * k + 1.0) * k


def body(n_sp, n_tp, n_chunk, heads, x_hbm, wq, wv, wf, wg, nx_hbm, room, extra, gain,
         mixed_out, cache_out, read_out,
         x, w, nx, qs, vs, cf, cb, kf_s, kb_s, gs, a_f, a_b, e_f, e_b, s_f, s_b, acc,
         inside, qc_hi, qc_lo, st_hi, st_lo, stage, got, stage2, got2, fin, nq_hi, nq_lo, nv, nown, ngate,
         load_sem, own_sem, ag_send, ag_recv, d2_send, d2_recv, p1_send, p1_recv, p2_send, p2_recv,
         p3_send, p3_recv):
    cols = heads * HD
    sp = lax.axis_index("sp")
    tp = lax.axis_index("tp")
    right = lax.rem(tp + 2, n_tp)
    left = lax.rem(tp + n_tp - 2, n_tp)
    far = lax.rem(tp + 4, n_tp)
    flip = 1 - 2 * lax.rem(tp, 2)
    mate = tp + flip

    barrier = pltpu.get_barrier_semaphore()
    for peer in (mate, left, right):
        pl.semaphore_signal(barrier, inc=1, device_id={"tp": peer}, device_id_type=MESH)

    def greet(i, c):
        pl.semaphore_signal(barrier, inc=1, device_id={"sp": lax.rem(sp + i, n_sp)}, device_id_type=MESH)
        return c

    lax.fori_loop(1, n_sp, greet, 0)

    def block(owner):
        return pl.ds(pl.multiple_of(owner * cols, cols), cols)

    def rows(j):
        return pl.ds(pl.multiple_of(j * B, B), B)

    loads = [pltpu.make_async_copy(x_hbm, x.at[:, block(tp)], load_sem.at[0]),
             pltpu.make_async_copy(nx_hbm, nx, load_sem.at[1]),
             pltpu.make_async_copy(wq, w.at[0], load_sem.at[2]),
             pltpu.make_async_copy(wv, w.at[1], load_sem.at[3]),
             pltpu.make_async_copy(wf.at[0], w.at[2], load_sem.at[4]),
             pltpu.make_async_copy(wf.at[1], w.at[3], load_sem.at[5]),
             pltpu.make_async_copy(wg, w.at[4], load_sem.at[6])]
    for load in loads:
        load.start()

    room_f = room[0:1, :]
    room_b = room[1:2, :]
    gain_row = gain[...]
    t_id = lax.broadcasted_iota(jnp.int32, (B, B), 0)
    s_id = lax.broadcasted_iota(jnp.int32, (B, B), 1)
    lower = t_id >= s_id
    upper = s_id >= t_id

    def silu_gain(g):
        return gain_row * (g / (1.0 + jnp.exp(-g)))

    def ring(kind, j):
        if kind == 0:
            src, to, r = block(tp), right, rows(j)
        elif kind == 1:
            src, to, r = block(tp), left, rows(j)
        elif kind == 2:
            src, to, r = block(left), right, pl.ds(pl.multiple_of(j * B, B), B // 2)
        else:
            src, to, r = block(right), left, pl.ds(pl.multiple_of(j * B + B // 2, B // 2), B // 2)
        return pltpu.make_async_remote_copy(
            src_ref=x.at[r, src], dst_ref=x.at[r, src], send_sem=ag_send.at[kind, j],
            recv_sem=ag_recv.at[kind, j], device_id={"tp": to}, device_id_type=MESH)

    def ring_in(kind, j):
        if kind == 0:
            src, r = block(left), rows(j)
        elif kind == 1:
            src, r = block(right), rows(j)
        elif kind == 2:
            src, r = block(far), pl.ds(pl.multiple_of(j * B, B), B // 2)
        else:
            src, r = block(far), pl.ds(pl.multiple_of(j * B + B // 2, B // 2), B // 2)
        return pltpu.make_async_remote_copy(
            src_ref=x.at[r, src], dst_ref=x.at[r, src], send_sem=ag_send.at[kind, j],
            recv_sem=ag_recv.at[kind, j], device_id={"tp": left}, device_id_type=MESH)

    def pair(kind, j, owner):
        return pltpu.make_async_remote_copy(
            src_ref=x.at[rows(j), block(owner)], dst_ref=x.at[rows(j), block(owner)],
            send_sem=d2_send.at[kind, j], recv_sem=d2_recv.at[kind, j],
            device_id={"tp": mate}, device_id_type=MESH)

    def pair_own(owner):
        return pltpu.make_async_remote_copy(
            src_ref=x.at[:, block(owner)], dst_ref=x.at[:, block(owner)],
            send_sem=own_sem.at[0], recv_sem=own_sem.at[1],
            device_id={"tp": mate}, device_id_type=MESH)

    for load in loads[1:]:
        load.wait()
    new = nx[...]
    nq_v = nn(new, w[0]).astype(BF16)
    nv[...] = nn(new, w[1]).astype(BF16)
    nf = room_f / (1.0 + jnp.exp(nn(new, w[2])))
    nb = room_b / (1.0 + jnp.exp(nn(new, w[3])))
    ngate[...] = silu_gain(nn(new, w[4]))
    nqf = nq_v.astype(F32)
    nq_hi[...], nq_lo[...] = split2(nqf * (1.0 - nf))
    nown[...] = nqf * (nf + nb)

    loads[0].wait()
    pl.semaphore_wait(barrier, n_sp + 2)

    pair_own(tp).start()
    for j in range(2):
        ring(0, j).start()
        ring(1, j).start()

    s_f[...] = jnp.zeros_like(s_f)
    s_b[...] = jnp.zeros_like(s_b)
    acc[...] = jnp.zeros_like(acc)

    def compute(c):
        r = rows(c)
        xc = x[r, :]
        fp = nn(xc, w[2])
        bp = nn(xc, w[3])
        kf = room_f / (1.0 + jnp.exp(fp))
        kb = room_b / (1.0 + jnp.exp(bp))
        kf_s[r, :] = kf
        kb_s[r, :] = kb
        vc = nn(xc, w[1]).astype(BF16)
        vs[r, :] = vc
        qs[r, :] = nn(xc, w[0]).astype(BF16)
        gs[r, :] = silu_gain(nn(xc, w[4]))
        tri_l = jnp.where(lower, 1.0, 0.0).astype(BF16)
        tri_u = jnp.where(upper, 1.0, 0.0).astype(BF16)
        lf_hi, lf_lo = split2(log_one_minus(kf))
        lb_hi, lb_lo = split2(log_one_minus(kb))
        wfc = nn(tri_l, lf_hi) + nn(tri_l, lf_lo)
        wbc = nn(tri_u, lb_hi) + nn(tri_u, lb_lo)
        ones = jnp.ones((B, HD), BF16)
        for h in range(heads):
            hs = slice(h * HD, (h + 1) * HD)
            ex = extra[h:h + 1, r]
            el_hi, el_lo = split2(jnp.where(lower, ex, 0.0))
            eu_hi, eu_lo = split2(jnp.where(upper, ex, 0.0))
            wfh = wfc[:, hs] + nn(el_hi, ones) + nn(el_lo, ones)
            wbh = wbc[:, hs] + nn(eu_hi, ones) + nn(eu_lo, ones)
            cf[r, hs] = wfh
            cb[r, hs] = wbh
            end_f = wfh[B - 1:B, :]
            end_b = wbh[0:1, :]
            ke_f = (kf[:, hs] * jnp.exp(end_f - wfh)).astype(BF16)
            ke_b = (kb[:, hs] * jnp.exp(end_b - wbh)).astype(BF16)
            af = tn(vc[:, hs], ke_f)
            ab = tn(vc[:, hs], ke_b)
            a_f[c, h] = af
            a_b[c, h] = ab
            e_f[c, h] = jnp.broadcast_to(jnp.exp(end_f), (8, HD))
            e_b[c, h] = jnp.broadcast_to(jnp.exp(end_b), (8, HD))
            s_f[h] = s_f[h] * jnp.exp(end_f) + af
            s_b[h] = s_b[h] + jnp.exp(acc[1, h, 0:1, :]) * ab
            acc[0, h] = acc[0, h] + end_f
            acc[1, h] = acc[1, h] + end_b

    def step(j, carry):
        @pl.when(j < n_chunk)
        def _():
            ring_in(0, j).wait_recv()
            ring_in(1, j).wait_recv()
            ring(2, j).start()
            ring(3, j).start()
            pair(0, j, left).start()
            pair(1, j, right).start()

        @pl.when(j + 2 < n_chunk)
        def _():
            ring(0, j + 2).start()
            ring(1, j + 2).start()

        @pl.when((j >= 1) & (j <= n_chunk))
        def _():
            ring_in(2, j - 1).wait_recv()
            ring_in(3, j - 1).wait_recv()
            pair(2, j - 1, far).start()

        @pl.when(j == 2)
        def _():
            pair_own(mate).wait_recv()

        @pl.when(j >= 2)
        def _():
            c = j - 2
            pair(0, c, left + flip).wait_recv()
            pair(1, c, right + flip).wait_recv()
            pair(2, c, far + flip).wait_recv()
            compute(c)

        return carry

    lax.fori_loop(0, n_chunk + 2, step, 0)

    per = n_sp // heads
    r_id = lax.broadcasted_iota(jnp.int32, (8, HD), 0)
    for h in range(heads):
        at = slice(h * per, (h + 1) * per)
        stage[at, 0] = s_f[h].reshape(per, 8, HD)
        stage[at, 1] = s_b[h].reshape(per, 8, HD)
        both = jnp.where(r_id == 0, acc[0, h], acc[1, h])
        stage[at, 2] = jnp.broadcast_to(both[None], (per, 8, HD))
    got[sp] = stage[sp]

    def send1(i, to, frm):
        return pltpu.make_async_remote_copy(
            src_ref=stage.at[to], dst_ref=got.at[frm], send_sem=p1_send.at[i], recv_sem=p1_recv.at[frm],
            device_id={"sp": to}, device_id_type=MESH)

    def send2(i, to, frm):
        return pltpu.make_async_remote_copy(
            src_ref=stage2.at[to], dst_ref=got2.at[frm], send_sem=p2_send.at[i], recv_sem=p2_recv.at[frm],
            device_id={"sp": to}, device_id_type=MESH)

    def send3(i, to, frm):
        return pltpu.make_async_remote_copy(
            src_ref=fin.at[sp], dst_ref=fin.at[frm], send_sem=p3_send.at[i], recv_sem=p3_recv.at[frm],
            device_id={"sp": to}, device_id_type=MESH)

    def spread(send):
        def one(i, c):
            send(i, lax.rem(sp + i, n_sp), sp).start()
            return c
        lax.fori_loop(1, n_sp, one, 0)

    def collect(send):
        def one(i, c):
            frm = lax.rem(sp + n_sp - i, n_sp)
            send(i, frm, frm).wait_recv()
            return c
        lax.fori_loop(1, n_sp, one, 0)

    def drain(send):
        def one(i, c):
            send(i, lax.rem(sp + i, n_sp), sp).wait_send()
            return c
        lax.fori_loop(1, n_sp, one, 0)

    spread(send1)

    def scores(c, carry):
        r = rows(c)
        for h in range(heads):
            hs = slice(h * HD, (h + 1) * HD)
            wfh = cf[r, hs]
            wbh = cb[r, hs]
            mid_f = wfh[B // 2:B // 2 + 1, :]
            mid_b = wbh[B // 2 - 1:B // 2, :]
            q = qs[r, hs].astype(F32)
            qi_f = (q * jnp.exp(wfh - mid_f)).astype(BF16)
            qi_b = (q * jnp.exp(wbh - mid_b)).astype(BF16)
            ki_f = (kf_s[r, hs] * jnp.exp(mid_f - wfh)).astype(BF16)
            ki_b = (kb_s[r, hs] * jnp.exp(mid_b - wbh)).astype(BF16)
            sc = jnp.where(lower, nt(qi_f, ki_f), 0.0) + jnp.where(upper, nt(qi_b, ki_b), 0.0)
            inside[r, hs] = nn(sc.astype(BF16), vs[r, hs])
            qc_hi[h, r, 0:HD], qc_lo[h, r, 0:HD] = split2(q * jnp.exp(wfh))
            qc_hi[h, r, HD:2 * HD], qc_lo[h, r, HD:2 * HD] = split2(q * jnp.exp(wbh))
        return carry

    half = n_chunk // 2
    lax.fori_loop(0, half, scores, 0)
    collect(send1)

    def decay(q, at):
        return jnp.exp(got[q, 2, at:at + 1, :])

    run = jnp.zeros((8, HD), F32)
    before = []
    for q in range(n_sp):
        before.append(run)
        run = run * decay(q, 0) + got[q, 0]
    fin[sp] = run
    run = jnp.zeros((8, HD), F32)
    for q in reversed(range(n_sp)):
        stage2[q, 0] = before[q]
        stage2[q, 1] = run
        run = run * decay(q, 1) + got[q, 1]
    got2[sp] = stage2[sp]
    spread(send2)
    spread(send3)

    lax.fori_loop(half, n_chunk, scores, 0)
    collect(send2)

    for h in range(heads):
        run = got2[h * per:(h + 1) * per, 0].reshape(HD, HD)
        for c in range(n_chunk):
            st_hi[h, c, :, 0:HD], st_lo[h, c, :, 0:HD] = split2(run)
            run = run * e_f[c, h, 0:1, :] + a_f[c, h]
        run = got2[h * per:(h + 1) * per, 1].reshape(HD, HD)
        for c in reversed(range(n_chunk)):
            st_hi[h, c, :, HD:2 * HD], st_lo[h, c, :, HD:2 * HD] = split2(run)
            run = run * e_b[c, h, 0:1, :] + a_b[c, h]

    def norm(mix, scale):
        return (mix * lax.rsqrt(jnp.mean(mix * mix, axis=-1, keepdims=True) + EPS) * scale).astype(BF16)

    def finish(c, carry):
        r = rows(c)
        for h in range(heads):
            hs = slice(h * HD, (h + 1) * HD)
            mix = (inside[r, hs] + nt(qc_lo[h, r, :], st_hi[h, c]) + nt(qc_hi[h, r, :], st_lo[h, c])
                   + nt(qc_hi[h, r, :], st_hi[h, c]))
            mixed_out[r, hs] = norm(mix, gs[r, hs])
        return carry

    lax.fori_loop(0, n_chunk, finish, 0)

    collect(send3)
    for h in range(heads):
        hs = slice(h * HD, (h + 1) * HD)
        last = fin[h * per:(h + 1) * per].reshape(HD, HD)
        cached = last.astype(BF16)
        cache_out[h] = last.T.astype(BF16)
        own = jnp.sum(nown[:, hs], axis=-1, keepdims=True) * nv[:, hs].astype(F32)
        read_out[:, hs] = norm(nt(nq_lo[:, hs], cached) + nt(nq_hi[:, hs], cached) + own, ngate[:, hs])

    def settle(j, c):
        for kind in range(4):
            ring(kind, j).wait_send()
        pair(0, j, left).wait_send()
        pair(1, j, right).wait_send()
        pair(2, j, far).wait_send()
        return c

    lax.fori_loop(0, n_chunk, settle, 0)
    pair_own(tp).wait_send()
    drain(send1)
    drain(send2)
    drain(send3)


def solution(mesh):
    n_sp, n_tp = mesh.shape["sp"], mesh.shape["tp"]

    def per_device(inputs, w_query, w_value, w_forget, w_gate, gate_room, extra_decay, out_gain, new_inputs):
        tokens, cols = inputs.shape
        depth = w_query.shape[0]
        heads = extra_decay.shape[0]
        fresh = new_inputs.shape[0]
        chunks = tokens // B
        anyspace = pl.BlockSpec(memory_space=pl.ANY)
        vmem = pl.BlockSpec(memory_space=pltpu.VMEM)

        def kernel(*refs):
            body(n_sp, n_tp, chunks, heads, *refs)

        dma = pltpu.SemaphoreType.DMA
        return pl.pallas_call(
            kernel,
            out_shape=(jax.ShapeDtypeStruct((tokens, cols), BF16),
                       jax.ShapeDtypeStruct((heads, HD, HD), BF16),
                       jax.ShapeDtypeStruct((fresh, cols), BF16)),
            in_specs=[anyspace] * 6 + [vmem] * 3,
            out_specs=(vmem, vmem, vmem),
            scratch_shapes=[
                pltpu.VMEM((tokens, depth), BF16),
                pltpu.VMEM((5, depth, cols), BF16),
                pltpu.VMEM((fresh, depth), BF16),
                pltpu.VMEM((tokens, cols), BF16),
                pltpu.VMEM((tokens, cols), BF16),
                pltpu.VMEM((tokens, cols), F32),
                pltpu.VMEM((tokens, cols), F32),
                pltpu.VMEM((tokens, cols), F32),
                pltpu.VMEM((tokens, cols), F32),
                pltpu.VMEM((tokens, cols), F32),
                pltpu.VMEM((chunks, heads, HD, HD), F32),
                pltpu.VMEM((chunks, heads, HD, HD), F32),
                pltpu.VMEM((chunks, heads, 8, HD), F32),
                pltpu.VMEM((chunks, heads, 8, HD), F32),
                pltpu.VMEM((heads, HD, HD), F32),
                pltpu.VMEM((heads, HD, HD), F32),
                pltpu.VMEM((2, heads, 8, HD), F32),
                pltpu.VMEM((tokens, cols), F32),
                pltpu.VMEM((heads, tokens, 2 * HD), BF16),
                pltpu.VMEM((heads, tokens, 2 * HD), BF16),
                pltpu.VMEM((heads, chunks, HD, 2 * HD), BF16),
                pltpu.VMEM((heads, chunks, HD, 2 * HD), BF16),
                pltpu.VMEM((n_sp, 3, 8, HD), F32),
                pltpu.VMEM((n_sp, 3, 8, HD), F32),
                pltpu.VMEM((n_sp, 2, 8, HD), F32),
                pltpu.VMEM((n_sp, 2, 8, HD), F32),
                pltpu.VMEM((n_sp, 8, HD), F32),
                pltpu.VMEM((fresh, cols), BF16),
                pltpu.VMEM((fresh, cols), BF16),
                pltpu.VMEM((fresh, cols), BF16),
                pltpu.VMEM((fresh, cols), F32),
                pltpu.VMEM((fresh, cols), F32),
                dma((7,)), dma((2,)),
                dma((4, chunks)), dma((4, chunks)),
                dma((3, chunks)), dma((3, chunks)),
                dma((n_sp,)), dma((n_sp,)),
                dma((n_sp,)), dma((n_sp,)),
                dma((n_sp,)), dma((n_sp,)),
            ],
            compiler_params=pltpu.CompilerParams(collective_id=0, has_side_effects=True,
                                                 vmem_limit_bytes=60 * 1024 * 1024),
        )(inputs, w_query, w_value, w_forget, w_gate, new_inputs, gate_room, extra_decay, out_gain.reshape(1, cols))

    return jax.shard_map(
        per_device,
        mesh=mesh,
        in_specs=(P("sp", "tp"), P(None, "tp"), P(None, "tp"), P(None, None, "tp"), P(None, "tp"),
                  P(None, "tp"), P("tp", "sp"), P("tp"), P()),
        out_specs=(P("sp", "tp"), P("tp", None, None), P(None, "tp")),
        check_vma=False,
    )
```

profile of v0, /device:TPU:64, one launch (start us, length us, event | category | flops | bytes accessed | tf_op | source)
XLA Modules:
  0.0 74.5 jit_solution(14479288360978255557)
XLA Ops:
  0.6 69.0 %shard_map.112 = (bf16[1024,256]{1,0:T(8,128)(2,1)}, bf16[2,128,128]{2,1,0:T(8,128)(2,1)}, bf16[128,256]{1,0:T(8,128)(2,1)}) custom-call(bf16[1024,256]{1,0:T(8,128)(2,1)} %refs_0_.1, bf16[2048,256]{1,0:T(8,128)(2,1)} %refs_1_.1, bf16[2048,256]{1,0:T(8,128)(2,1)} %refs_2_.1, bf16[2,2048,256]{2,1,0:T(8,128)(2,1)} %refs_3_.1, bf16[2048,256]{1,0:T(8,128)(2,1)} %refs_4_.1, ...), custom_call_target="tpu_custom_call" | custom-call | tf_op jit(solution)/shard_map/pallas_call | solution.py:389
  69.7 1.9 %copy.15 = bf16[1024,256]{1,0:T(8,128)(2,1)} copy(bf16[1024,256]{1,0:T(8,128)(2,1)} %get-tuple-element.6) | data formatting | bytes 1048576
  71.5 1.5 %copy.16 = bf16[2,128,128]{2,1,0:T(8,128)(2,1)} copy(bf16[2,128,128]{2,1,0:T(8,128)(2,1)} %get-tuple-element.7) | data formatting | bytes 131072
  73.0 1.5 %copy.17 = bf16[128,256]{1,0:T(8,128)(2,1)} copy(bf16[128,256]{1,0:T(8,128)(2,1)} %get-tuple-element.8) | data formatting | bytes 131072
where the time goes:
time: 74.7 us; the launch traced here: 74.5 us
  Pallas kernels  69 us (92%)
  local copies, waits for them, and re-layouts  4.81 us (6%)
    pallas_call x1, Pallas kernels, per_device(): pl.pallas_call(kernel, out_shape=(jax.ShapeDtypeStruct((tokens, cols), BF...  69 us
    unnamed x3, local copies, waits for them, and re-layouts  4.81 us

commit v1 on v0

--- a/solution.py
+++ b/solution.py
@@ -9,6 +9,8 @@
 EPS = 1e-06
 B = 128
 HD = 128
+VM1 = 48
+NX = 4
 F32 = jnp.float32
 BF16 = jnp.bfloat16
 
@@ -37,10 +39,10 @@
     return -(s * k + 1.0) * k
 
 
-def body(n_sp, n_tp, n_chunk, heads, x_hbm, wq, wv, wf, wg, nx_hbm, room, extra, gain,
+def body(n_sp, n_tp, n_chunk, heads, x_hbm, wq, wv, wf, wg, nx_hbm, room_hbm, extra_hbm, gain_hbm,
          mixed_out, cache_out, read_out,
-         x, w, nx, qs, vs, cf, cb, kf_s, kb_s, gs, a_f, a_b, e_f, e_b, s_f, s_b, acc,
-         inside, qc_hi, qc_lo, st_hi, st_lo, stage, got, stage2, got2, fin, nq_hi, nq_lo, nv, nown, ngate,
+         x, w, nx, room, extra, gain, qs, vs, cf, cb, kf_s, kb_s, gs, a_f, a_b, e_f, e_b, s_f, s_b, acc,
+         inside, qc_hi, qc_lo, st_hi, st_lo, stage_f, stage_b, stage_d, got_f, got_b, got_d, stage2, got2, fin, nq_hi, nq_lo, nv, nown, ngate,
          load_sem, own_sem, ag_send, ag_recv, d2_send, d2_recv, p1_send, p1_recv, p2_send, p2_recv,
          p3_send, p3_recv):
     cols = heads * HD
@@ -68,26 +70,19 @@
     def rows(j):
         return pl.ds(pl.multiple_of(j * B, B), B)
 
-    loads = [pltpu.make_async_copy(x_hbm, x.at[:, block(tp)], load_sem.at[0]),
-             pltpu.make_async_copy(nx_hbm, nx, load_sem.at[1]),
-             pltpu.make_async_copy(wq, w.at[0], load_sem.at[2]),
-             pltpu.make_async_copy(wv, w.at[1], load_sem.at[3]),
-             pltpu.make_async_copy(wf.at[0], w.at[2], load_sem.at[4]),
-             pltpu.make_async_copy(wf.at[1], w.at[3], load_sem.at[5]),
-             pltpu.make_async_copy(wg, w.at[4], load_sem.at[6])]
+    loads = [pltpu.make_async_copy(src, dst, load_sem.at[i]) for i, (src, dst) in enumerate((
+        (x_hbm, x.at[:, block(tp)]), (room_hbm, room), (extra_hbm, extra), (wf.at[0], w.at[2]), (wf.at[1], w.at[3]),
+        (wv, w.at[1]), (gain_hbm, gain), (wq, w.at[0]), (wg, w.at[4]), (nx_hbm, nx)))]
     for load in loads:
         load.start()
 
-    room_f = room[0:1, :]
-    room_b = room[1:2, :]
-    gain_row = gain[...]
     t_id = lax.broadcasted_iota(jnp.int32, (B, B), 0)
     s_id = lax.broadcasted_iota(jnp.int32, (B, B), 1)
     lower = t_id >= s_id
     upper = s_id >= t_id
 
     def silu_gain(g):
-        return gain_row * (g / (1.0 + jnp.exp(-g)))
+        return gain[...] * (g / (1.0 + jnp.exp(-g)))
 
     def ring(kind, j):
         if kind == 0:
@@ -127,18 +122,6 @@
             send_sem=own_sem.at[0], recv_sem=own_sem.at[1],
             device_id={"tp": mate}, device_id_type=MESH)
 
-    for load in loads[1:]:
-        load.wait()
-    new = nx[...]
-    nq_v = nn(new, w[0]).astype(BF16)
-    nv[...] = nn(new, w[1]).astype(BF16)
-    nf = room_f / (1.0 + jnp.exp(nn(new, w[2])))
-    nb = room_b / (1.0 + jnp.exp(nn(new, w[3])))
-    ngate[...] = silu_gain(nn(new, w[4]))
-    nqf = nq_v.astype(F32)
-    nq_hi[...], nq_lo[...] = split2(nqf * (1.0 - nf))
-    nown[...] = nqf * (nf + nb)
-
     loads[0].wait()
     pl.semaphore_wait(barrier, n_sp + 2)
 
@@ -154,16 +137,12 @@
     def compute(c):
         r = rows(c)
         xc = x[r, :]
-        fp = nn(xc, w[2])
-        bp = nn(xc, w[3])
-        kf = room_f / (1.0 + jnp.exp(fp))
-        kb = room_b / (1.0 + jnp.exp(bp))
+        kf = room[0:1, :] / (1.0 + jnp.exp(nn(xc, w[2])))
+        kb = room[1:2, :] / (1.0 + jnp.exp(nn(xc, w[3])))
         kf_s[r, :] = kf
         kb_s[r, :] = kb
         vc = nn(xc, w[1]).astype(BF16)
         vs[r, :] = vc
-        qs[r, :] = nn(xc, w[0]).astype(BF16)
-        gs[r, :] = silu_gain(nn(xc, w[4]))
         tri_l = jnp.where(lower, 1.0, 0.0).astype(BF16)
         tri_u = jnp.where(upper, 1.0, 0.0).astype(BF16)
         lf_hi, lf_lo = split2(log_one_minus(kf))
@@ -182,9 +161,9 @@
             cb[r, hs] = wbh
             end_f = wfh[B - 1:B, :]
             end_b = wbh[0:1, :]
-            ke_f = (kf[:, hs] * jnp.exp(end_f - wfh)).astype(BF16)
+            ke_hi, ke_lo = split2(kf[:, hs] * jnp.exp(end_f - wfh))
             ke_b = (kb[:, hs] * jnp.exp(end_b - wbh)).astype(BF16)
-            af = tn(vc[:, hs], ke_f)
+            af = tn(vc[:, hs], ke_hi) + tn(vc[:, hs], ke_lo)
             ab = tn(vc[:, hs], ke_b)
             a_f[c, h] = af
             a_b[c, h] = ab
@@ -210,15 +189,11 @@
             ring(0, j + 2).start()
             ring(1, j + 2).start()
 
-        @pl.when((j >= 1) & (j <= n_chunk))
-        def _():
-            ring_in(2, j - 1).wait_recv()
-            ring_in(3, j - 1).wait_recv()
-            pair(2, j - 1, far).start()
-
         @pl.when(j == 2)
         def _():
             pair_own(mate).wait_recv()
+            for load in loads[1:6]:
+                load.wait()
 
         @pl.when(j >= 2)
         def _():
@@ -228,55 +203,79 @@
             pair(2, c, far + flip).wait_recv()
             compute(c)
 
+        @pl.when((j >= 1) & (j <= n_chunk))
+        def _():
+            ring_in(2, j - 1).wait_recv()
+            ring_in(3, j - 1).wait_recv()
+            pair(2, j - 1, far).start()
+
         return carry
 
     lax.fori_loop(0, n_chunk + 2, step, 0)
 
     per = n_sp // heads
-    r_id = lax.broadcasted_iota(jnp.int32, (8, HD), 0)
+    nz = n_sp // NX
+    r_id = lax.broadcasted_iota(jnp.int32, (2, HD), 0)
     for h in range(heads):
         at = slice(h * per, (h + 1) * per)
-        stage[at, 0] = s_f[h].reshape(per, 8, HD)
-        stage[at, 1] = s_b[h].reshape(per, 8, HD)
-        both = jnp.where(r_id == 0, acc[0, h], acc[1, h])
-        stage[at, 2] = jnp.broadcast_to(both[None], (per, 8, HD))
-    got[sp] = stage[sp]
-
-    def send1(i, to, frm):
-        return pltpu.make_async_remote_copy(
-            src_ref=stage.at[to], dst_ref=got.at[frm], send_sem=p1_send.at[i], recv_sem=p1_recv.at[frm],
-            device_id={"sp": to}, device_id_type=MESH)
-
-    def send2(i, to, frm):
-        return pltpu.make_async_remote_copy(
-            src_ref=stage2.at[to], dst_ref=got2.at[frm], send_sem=p2_send.at[i], recv_sem=p2_recv.at[frm],
-            device_id={"sp": to}, device_id_type=MESH)
-
-    def send3(i, to, frm):
-        return pltpu.make_async_remote_copy(
-            src_ref=fin.at[sp], dst_ref=fin.at[frm], send_sem=p3_send.at[i], recv_sem=p3_recv.at[frm],
-            device_id={"sp": to}, device_id_type=MESH)
-
-    def spread(send):
-        def one(i, c):
-            send(i, lax.rem(sp + i, n_sp), sp).start()
-            return c
-        lax.fori_loop(1, n_sp, one, 0)
-
-    def collect(send):
-        def one(i, c):
-            frm = lax.rem(sp + n_sp - i, n_sp)
-            send(i, frm, frm).wait_recv()
-            return c
-        lax.fori_loop(1, n_sp, one, 0)
-
-    def drain(send):
-        def one(i, c):
-            send(i, lax.rem(sp + i, n_sp), sp).wait_send()
-            return c
-        lax.fori_loop(1, n_sp, one, 0)
-
-    spread(send1)
+        stage_f[at] = s_f[h].reshape(per, 8, HD)
+        stage_b[at] = s_b[h].reshape(per, 8, HD).astype(BF16)
+        both = jnp.where(r_id == 0, acc[0, h, 0:2], acc[1, h, 0:2])
+        stage_d[at] = jnp.broadcast_to(both[None], (per, 2, HD))
+    got_f[sp] = stage_f[sp]
+    got_b[sp] = stage_b[sp]
+    got_d[sp] = stage_d[sp]
+
+    def other(i, sign):
+        m, n = i // NX, lax.rem(i, NX)
+        dz = nz // 2 + ((m + 1) // 2) * (1 - 2 * lax.rem(m, 2))
+        dx = NX // 2 + ((n + 1) // 2) * (1 - 2 * lax.rem(n, 2))
+        z, xx = sp // NX, lax.rem(sp, NX)
+        return lax.rem(z + sign * dz + 2 * nz, nz) * NX + lax.rem(xx + sign * dx + 2 * NX, NX)
+
+    def exchange(stages, gots, sends, recvs, whole=False):
+        def copies(i, to, frm):
+            return [pltpu.make_async_remote_copy(
+                src_ref=st.at[sp] if whole else st.at[to], dst_ref=gt.at[frm], send_sem=sends.at[n, i],
+                recv_sem=recvs.at[n, frm], device_id={"sp": to}, device_id_type=MESH)
+                for n, (st, gt) in enumerate(zip(stages, gots))]
+
+        def spread():
+            def one(i, c):
+                for copy in copies(i, other(i, 1), sp):
+                    copy.start()
+                return c
+            lax.fori_loop(0, n_sp - 1, one, 0)
+
+        def collect():
+            def one(i, c):
+                frm = other(i, -1)
+                for copy in copies(i, frm, frm):
+                    copy.wait_recv()
+                return c
+            lax.fori_loop(0, n_sp - 1, one, 0)
+
+        def drain():
+            def one(i, c):
+                for copy in copies(i, other(i, 1), sp):
+                    copy.wait_send()
+                return c
+            lax.fori_loop(0, n_sp - 1, one, 0)
+
+        return spread, collect, drain
+
+    spread1, collect1, drain1 = exchange((stage_d, stage_f, stage_b), (got_d, got_f, got_b), p1_send, p1_recv)
+    spread2, collect2, drain2 = exchange((stage2,), (got2,), p2_send, p2_recv)
+    spread3, collect3, drain3 = exchange((fin,), (fin,), p3_send, p3_recv, whole=True)
+
+    spread1()
+
+    def queries(c, carry):
+        r = rows(c)
+        xc = x[r, :]
+        qs[r, :] = nn(xc, w[0]).astype(BF16)
+        gs[r, :] = silu_gain(nn(xc, w[4]))
+        return carry
 
     def scores(c, carry):
         r = rows(c)
@@ -297,30 +296,57 @@
             qc_hi[h, r, HD:2 * HD], qc_lo[h, r, HD:2 * HD] = split2(q * jnp.exp(wbh))
         return carry
 
-    half = n_chunk // 2
-    lax.fori_loop(0, half, scores, 0)
-    collect(send1)
+    def inner(c, carry):
+        queries(c, 0)
+        return scores(c, 0)
+
+    for load in loads[6:]:
+        load.wait()
+    early = n_chunk // 2
+    lax.fori_loop(0, early, inner, 0)
+    new = nx[...]
+    nqf = nn(new, w[0]).astype(BF16).astype(F32)
+    nv[...] = nn(new, w[1]).astype(BF16)
+    nf = room[0:1, :] / (1.0 + jnp.exp(nn(new, w[2])))
+    nb = room[1:2, :] / (1.0 + jnp.exp(nn(new, w[3])))
+    ngate[...] = silu_gain(nn(new, w[4]))
+    nq_hi[...], nq_lo[...] = split2(nqf * (1.0 - nf))
+    nown[...] = nqf * (nf + nb)
+
+    collect1()
 
     def decay(q, at):
-        return jnp.exp(got[q, 2, at:at + 1, :])
+        return jnp.exp(got_d[q, at:at + 1, :])
 
     run = jnp.zeros((8, HD), F32)
     before = []
     for q in range(n_sp):
         before.append(run)
-        run = run * decay(q, 0) + got[q, 0]
-    fin[sp] = run
+        run = run * decay(q, 0) + got_f[q]
+    fin[sp] = run.astype(BF16)
     run = jnp.zeros((8, HD), F32)
     for q in reversed(range(n_sp)):
         stage2[q, 0] = before[q]
         stage2[q, 1] = run
-        run = run * decay(q, 1) + got[q, 1]
+        run = run * decay(q, 1) + got_b[q].astype(F32)
     got2[sp] = stage2[sp]
-    spread(send2)
-    spread(send3)
-
-    lax.fori_loop(half, n_chunk, scores, 0)
-    collect(send2)
+    spread2()
+    spread3()
+
+    lax.fori_loop(early, n_chunk, inner, 0)
+
+    def settle(j, c):
+        for kind in range(4):
+            ring(kind, j).wait_send()
+        pair(0, j, left).wait_send()
+        pair(1, j, right).wait_send()
+        pair(2, j, far).wait_send()
+        return c
+
+    lax.fori_loop(0, n_chunk, settle, 0)
+    pair_own(tp).wait_send()
+    drain1()
+    collect2()
 
     for h in range(heads):
         run = got2[h * per:(h + 1) * per, 0].reshape(HD, HD)
@@ -344,30 +370,19 @@
             mixed_out[r, hs] = norm(mix, gs[r, hs])
         return carry
 
-    lax.fori_loop(0, n_chunk, finish, 0)
-
-    collect(send3)
+    lax.fori_loop(0, n_chunk, finish, 0, unroll=2)
+
+    collect3()
     for h in range(heads):
         hs = slice(h * HD, (h + 1) * HD)
-        last = fin[h * per:(h + 1) * per].reshape(HD, HD)
+        last = fin[h * per:(h + 1) * per].astype(F32).reshape(HD, HD)
         cached = last.astype(BF16)
         cache_out[h] = last.T.astype(BF16)
         own = jnp.sum(nown[:, hs], axis=-1, keepdims=True) * nv[:, hs].astype(F32)
         read_out[:, hs] = norm(nt(nq_lo[:, hs], cached) + nt(nq_hi[:, hs], cached) + own, ngate[:, hs])
 
-    def settle(j, c):
-        for kind in range(4):
-            ring(kind, j).wait_send()
-        pair(0, j, left).wait_send()
-        pair(1, j, right).wait_send()
-        pair(2, j, far).wait_send()
-        return c
-
-    lax.fori_loop(0, n_chunk, settle, 0)
-    pair_own(tp).wait_send()
-    drain(send1)
-    drain(send2)
-    drain(send3)
+    drain2()
+    drain3()
 
 
 def solution(mesh):
@@ -379,24 +394,27 @@
         heads = extra_decay.shape[0]
         fresh = new_inputs.shape[0]
         chunks = tokens // B
-        anyspace = pl.BlockSpec(memory_space=pl.ANY)
+        hbm = pl.BlockSpec(memory_space=pltpu.HBM)
         vmem = pl.BlockSpec(memory_space=pltpu.VMEM)
 
         def kernel(*refs):
             body(n_sp, n_tp, chunks, heads, *refs)
 
         dma = pltpu.SemaphoreType.DMA
-        return pl.pallas_call(
+        done = pl.pallas_call(
             kernel,
             out_shape=(jax.ShapeDtypeStruct((tokens, cols), BF16),
                        jax.ShapeDtypeStruct((heads, HD, HD), BF16),
                        jax.ShapeDtypeStruct((fresh, cols), BF16)),
-            in_specs=[anyspace] * 6 + [vmem] * 3,
+            in_specs=[hbm] * 9,
             out_specs=(vmem, vmem, vmem),
             scratch_shapes=[
                 pltpu.VMEM((tokens, depth), BF16),
                 pltpu.VMEM((5, depth, cols), BF16),
                 pltpu.VMEM((fresh, depth), BF16),
+                pltpu.VMEM((2, cols), F32),
+                pltpu.VMEM((heads, tokens), F32),
+                pltpu.VMEM((1, cols), F32),
                 pltpu.VMEM((tokens, cols), BF16),
                 pltpu.VMEM((tokens, cols), BF16),
                 pltpu.VMEM((tokens, cols), F32),
@@ -416,26 +434,48 @@
                 pltpu.VMEM((heads, tokens, 2 * HD), BF16),
                 pltpu.VMEM((heads, chunks, HD, 2 * HD), BF16),
                 pltpu.VMEM((heads, chunks, HD, 2 * HD), BF16),
-                pltpu.VMEM((n_sp, 3, 8, HD), F32),
-                pltpu.VMEM((n_sp, 3, 8, HD), F32),
+                pltpu.VMEM((n_sp, 8, HD), F32),
+                pltpu.VMEM((n_sp, 8, HD), BF16),
+                pltpu.VMEM((n_sp, 2, HD), F32),
+                pltpu.VMEM((n_sp, 8, HD), F32),
+                pltpu.VMEM((n_sp, 8, HD), BF16),
+                pltpu.VMEM((n_sp, 2, HD), F32),
                 pltpu.VMEM((n_sp, 2, 8, HD), F32),
                 pltpu.VMEM((n_sp, 2, 8, HD), F32),
-                pltpu.VMEM((n_sp, 8, HD), F32),
+                pltpu.VMEM((n_sp, 8, HD), BF16),
                 pltpu.VMEM((fresh, cols), BF16),
                 pltpu.VMEM((fresh, cols), BF16),
                 pltpu.VMEM((fresh, cols), BF16),
                 pltpu.VMEM((fresh, cols), F32),
                 pltpu.VMEM((fresh, cols), F32),
-                dma((7,)), dma((2,)),
+                dma((10,)), dma((2,)),
                 dma((4, chunks)), dma((4, chunks)),
                 dma((3, chunks)), dma((3, chunks)),
-                dma((n_sp,)), dma((n_sp,)),
-                dma((n_sp,)), dma((n_sp,)),
-                dma((n_sp,)), dma((n_sp,)),
+                dma((3, n_sp)), dma((3, n_sp)),
+                dma((1, n_sp)), dma((1, n_sp)),
+                dma((1, n_sp)), dma((1, n_sp)),
             ],
             compiler_params=pltpu.CompilerParams(collective_id=0, has_side_effects=True,
-                                                 vmem_limit_bytes=60 * 1024 * 1024),
-        )(inputs, w_query, w_value, w_forget, w_gate, new_inputs, gate_room, extra_decay, out_gain.reshape(1, cols))
+                                                 vmem_limit_bytes=VM1 * 1024 * 1024),
+        )(*(pltpu.with_memory_space_constraint(a, pltpu.HBM) for a in (
+            inputs, w_query, w_value, w_forget, w_gate, new_inputs, gate_room, extra_decay, out_gain.reshape(1, cols))))
+
+        def put(a, b, c, a_out, b_out, c_out, sems):
+            copies = [pltpu.make_async_copy(s, d, sems.at[i])
+                      for i, (s, d) in enumerate(((a, a_out), (b, b_out), (c, c_out)))]
+            for copy in copies:
+                copy.start()
+            for copy in copies:
+                copy.wait()
+
+        return pl.pallas_call(
+            put,
+            out_shape=tuple(jax.ShapeDtypeStruct(d.shape, d.dtype) for d in done),
+            in_specs=[vmem] * 3,
+            out_specs=(hbm,) * 3,
+            scratch_shapes=[dma((3,))],
+            compiler_params=pltpu.CompilerParams(vmem_limit_bytes=4 * 1024 * 1024),
+        )(*done)
 
     return jax.shard_map(
         per_device,

time: 74.7 us -> 65.9 us (0.88)
  the two profiles are of different devices: /device:TPU:64 before, /device:TPU:1 now
where the time goes in v1:
time: 65.9 us; the launch traced here: 65.8 us
  Pallas kernels  65.1 us (99%)
    pallas_call x1, Pallas kernels, per_device(): pl.pallas_call(kernel, out_shape=(jax.ShapeDtypeStruct((tokens, cols), BF...  64.3 us

profile of v1, /device:TPU:1, one launch (start us, length us, event | category | flops | bytes accessed | tf_op | source)
XLA Modules:
  0.0 65.8 jit_solution(7918079319115873215)
XLA Ops:
  0.6 64.3 %shard_map.112 = (bf16[1024,256]{1,0:T(8,128)(2,1)S(1)}, bf16[2,128,128]{2,1,0:T(8,128)(2,1)S(1)}, bf16[128,256]{1,0:T(8,128)(2,1)S(1)}) custom-call(bf16[1024,256]{1,0:T(8,128)(2,1)} %refs_0_.1, bf16[2048,256]{1,0:T(8,128)(2,1)} %refs_1_.1, bf16[2048,256]{1,0:T(8,128)(2,1)} %refs_2_.1, bf16[2,2048,256]{2,1,0:T(8,128)(2,1)} %refs_3_.1, ...), custom_call_target="tpu_custom_call" | custom-call | tf_op jit(solution)/shard_map/pallas_call | solution.py:404
  64.9 0.9 %shard_map.113 = (bf16[1024,256]{1,0:T(8,128)(2,1)}, bf16[2,128,128]{2,1,0:T(8,128)(2,1)}, bf16[128,256]{1,0:T(8,128)(2,1)}) custom-call(bf16[1024,256]{1,0:T(8,128)(2,1)S(1)} %get-tuple-element.6.a, bf16[2,128,128]{2,1,0:T(8,128)(2,1)S(1)} %get-tuple-element.7.b, bf16[128,256]{1,0:T(8,128)(2,1)S(1)} %get-tuple-element.8.c), custom_call_target="tpu_custom_call" | custom-call | tf_op jit(solution)/shard_map/pallas_call | solution.py:471

commit v2 on v1

--- a/solution.py
+++ b/solution.py
@@ -10,6 +10,7 @@
 B = 128
 HD = 128
 VM1 = 48
+LEAD = 3
 NX = 4
 F32 = jnp.float32
 BF16 = jnp.bfloat16
@@ -41,9 +42,9 @@
 
 def body(n_sp, n_tp, n_chunk, heads, x_hbm, wq, wv, wf, wg, nx_hbm, room_hbm, extra_hbm, gain_hbm,
          mixed_out, cache_out, read_out,
-         x, w, nx, room, extra, gain, qs, vs, cf, cb, kf_s, kb_s, gs, a_f, a_b, e_f, e_b, s_f, s_b, acc,
+         x, w, nx, part, room, extra, gain, qs, vs, cf, cb, kf_s, kb_s, gs, a_f, a_b, e_f, e_b, s_f, s_b, acc,
          inside, qc_hi, qc_lo, st_hi, st_lo, stage_f, stage_b, stage_d, got_f, got_b, got_d, stage2, got2, fin, nq_hi, nq_lo, nv, nown, ngate,
-         load_sem, own_sem, ag_send, ag_recv, d2_send, d2_recv, p1_send, p1_recv, p2_send, p2_recv,
+         load_sem, own_sem, out_sem, near_in, far_in, mate_near, mate_far, p1_send, p1_recv, p2_send, p2_recv,
          p3_send, p3_recv):
     cols = heads * HD
     sp = lax.axis_index("sp")
@@ -84,51 +85,61 @@
     def silu_gain(g):
         return gain[...] * (g / (1.0 + jnp.exp(-g)))
 
-    def ring(kind, j):
-        if kind == 0:
-            src, to, r = block(tp), right, rows(j)
-        elif kind == 1:
-            src, to, r = block(tp), left, rows(j)
-        elif kind == 2:
-            src, to, r = block(left), right, pl.ds(pl.multiple_of(j * B, B), B // 2)
-        else:
-            src, to, r = block(right), left, pl.ds(pl.multiple_of(j * B + B // 2, B // 2), B // 2)
+    def half(j, k):
+        return pl.ds(pl.multiple_of(j * B + k * (B // 2), B // 2), B // 2)
+
+    def chip(owner):
+        return pl.ds(pl.multiple_of((owner // 2) * (2 * cols), 2 * cols), 2 * cols)
+
+    def push(r, c, to, out, inn):
         return pltpu.make_async_remote_copy(
-            src_ref=x.at[r, src], dst_ref=x.at[r, src], send_sem=ag_send.at[kind, j],
-            recv_sem=ag_recv.at[kind, j], device_id={"tp": to}, device_id_type=MESH)
-
-    def ring_in(kind, j):
-        if kind == 0:
-            src, r = block(left), rows(j)
-        elif kind == 1:
-            src, r = block(right), rows(j)
-        elif kind == 2:
-            src, r = block(far), pl.ds(pl.multiple_of(j * B, B), B // 2)
-        else:
-            src, r = block(far), pl.ds(pl.multiple_of(j * B + B // 2, B // 2), B // 2)
-        return pltpu.make_async_remote_copy(
-            src_ref=x.at[r, src], dst_ref=x.at[r, src], send_sem=ag_send.at[kind, j],
-            recv_sem=ag_recv.at[kind, j], device_id={"tp": left}, device_id_type=MESH)
-
-    def pair(kind, j, owner):
-        return pltpu.make_async_remote_copy(
-            src_ref=x.at[rows(j), block(owner)], dst_ref=x.at[rows(j), block(owner)],
-            send_sem=d2_send.at[kind, j], recv_sem=d2_recv.at[kind, j],
-            device_id={"tp": mate}, device_id_type=MESH)
+            src_ref=x.at[r, c], dst_ref=x.at[r, c], send_sem=out, recv_sem=inn,
+            device_id={"tp": to}, device_id_type=MESH)
+
+    def send_own(j):
+        push(rows(j), block(tp), right, out_sem.at[0], near_in.at[j]).start()
+        push(rows(j), block(tp), left, out_sem.at[0], near_in.at[j]).start()
+
+    def pass_near(j):
+        push(half(j, 0), block(left), right, out_sem.at[1], far_in.at[j]).start()
+        push(half(j, 1), block(right), left, out_sem.at[1], far_in.at[j]).start()
+        push(rows(j), block(left), mate, out_sem.at[2], mate_near.at[j]).start()
+        push(rows(j), block(right), mate, out_sem.at[2], mate_near.at[j]).start()
+
+    def pass_far(j):
+        push(rows(j), block(far), mate, out_sem.at[3], mate_far.at[j]).start()
+
+    whole = pl.ds(0, n_chunk * B)
 
     def pair_own(owner):
-        return pltpu.make_async_remote_copy(
-            src_ref=x.at[:, block(owner)], dst_ref=x.at[:, block(owner)],
-            send_sem=own_sem.at[0], recv_sem=own_sem.at[1],
-            device_id={"tp": mate}, device_id_type=MESH)
+        return push(whole, block(owner), mate, own_sem.at[0], own_sem.at[1])
 
     loads[0].wait()
     pl.semaphore_wait(barrier, n_sp + 2)
 
     pair_own(tp).start()
-    for j in range(2):
-        ring(0, j).start()
-        ring(1, j).start()
+    for j in range(LEAD):
+        send_own(j)
+
+    kinds = (2, 3, 1)
+
+    def own_part(c, carry):
+        r = rows(c)
+        xc = x[r, chip(tp)]
+        for n, i in enumerate(kinds):
+            part[n, r, :] = nn(xc, w[i, chip(tp), :])
+        return carry
+
+    def near_part(c):
+        r = rows(c)
+        xl, xr = x[r, chip(left)], x[r, chip(right)]
+        for n, i in enumerate(kinds):
+            part[n, r, :] += nn(xl, w[i, chip(left), :]) + nn(xr, w[i, chip(right), :])
+
+    for load in loads[1:6]:
+        load.wait()
+    pair_own(mate).wait_recv()
+    lax.fori_loop(0, n_chunk, own_part, 0)
 
     s_f[...] = jnp.zeros_like(s_f)
     s_b[...] = jnp.zeros_like(s_b)
@@ -136,12 +147,12 @@
 
     def compute(c):
         r = rows(c)
-        xc = x[r, :]
-        kf = room[0:1, :] / (1.0 + jnp.exp(nn(xc, w[2])))
-        kb = room[1:2, :] / (1.0 + jnp.exp(nn(xc, w[3])))
+        xc = x[r, chip(far)]
+        kf = room[0:1, :] / (1.0 + jnp.exp(part[0, r, :] + nn(xc, w[2, chip(far), :])))
+        kb = room[1:2, :] / (1.0 + jnp.exp(part[1, r, :] + nn(xc, w[3, chip(far), :])))
         kf_s[r, :] = kf
         kb_s[r, :] = kb
-        vc = nn(xc, w[1]).astype(BF16)
+        vc = (part[2, r, :] + nn(xc, w[1, chip(far), :])).astype(BF16)
         vs[r, :] = vc
         tri_l = jnp.where(lower, 1.0, 0.0).astype(BF16)
         tri_u = jnp.where(upper, 1.0, 0.0).astype(BF16)
@@ -177,37 +188,26 @@
     def step(j, carry):
         @pl.when(j < n_chunk)
         def _():
-            ring_in(0, j).wait_recv()
-            ring_in(1, j).wait_recv()
-            ring(2, j).start()
-            ring(3, j).start()
-            pair(0, j, left).start()
-            pair(1, j, right).start()
-
-        @pl.when(j + 2 < n_chunk)
+            push(rows(j), chip(left), left, out_sem.at[0], near_in.at[j]).wait_recv()
+            pass_near(j)
+
+        @pl.when(j + LEAD < n_chunk)
         def _():
-            ring(0, j + 2).start()
-            ring(1, j + 2).start()
-
-        @pl.when(j == 2)
+            send_own(j + LEAD)
+
+        @pl.when((j >= 1) & (j <= n_chunk))
         def _():
-            pair_own(mate).wait_recv()
-            for load in loads[1:6]:
-                load.wait()
+            c = j - 1
+            push(rows(c), chip(left), mate, out_sem.at[2], mate_near.at[c]).wait_recv()
+            near_part(c)
+            push(rows(c), block(far), left, out_sem.at[1], far_in.at[c]).wait_recv()
+            pass_far(c)
 
         @pl.when(j >= 2)
         def _():
             c = j - 2
-            pair(0, c, left + flip).wait_recv()
-            pair(1, c, right + flip).wait_recv()
-            pair(2, c, far + flip).wait_recv()
+            push(rows(c), block(far), mate, out_sem.at[3], mate_far.at[c]).wait_recv()
             compute(c)
-
-        @pl.when((j >= 1) & (j <= n_chunk))
-        def _():
-            ring_in(2, j - 1).wait_recv()
-            ring_in(3, j - 1).wait_recv()
-            pair(2, j - 1, far).start()
 
         return carry
 
@@ -226,41 +226,39 @@
     got_b[sp] = stage_b[sp]
     got_d[sp] = stage_d[sp]
 
-    def other(i, sign):
+    def other(i):
         m, n = i // NX, lax.rem(i, NX)
         dz = nz // 2 + ((m + 1) // 2) * (1 - 2 * lax.rem(m, 2))
         dx = NX // 2 + ((n + 1) // 2) * (1 - 2 * lax.rem(n, 2))
         z, xx = sp // NX, lax.rem(sp, NX)
-        return lax.rem(z + sign * dz + 2 * nz, nz) * NX + lax.rem(xx + sign * dx + 2 * NX, NX)
+        return lax.rem(z + dz, nz) * NX + lax.rem(xx + dx, NX)
 
     def exchange(stages, gots, sends, recvs, whole=False):
-        def copies(i, to, frm):
+        def copies(to, frm):
             return [pltpu.make_async_remote_copy(
-                src_ref=st.at[sp] if whole else st.at[to], dst_ref=gt.at[frm], send_sem=sends.at[n, i],
-                recv_sem=recvs.at[n, frm], device_id={"sp": to}, device_id_type=MESH)
+                src_ref=st.at[sp] if whole else st.at[to], dst_ref=gt.at[frm], send_sem=sends.at[n],
+                recv_sem=recvs.at[n], device_id={"sp": to}, device_id_type=MESH)
                 for n, (st, gt) in enumerate(zip(stages, gots))]
 
         def spread():
             def one(i, c):
-                for copy in copies(i, other(i, 1), sp):
+                for copy in copies(other(i), sp):
                     copy.start()
                 return c
             lax.fori_loop(0, n_sp - 1, one, 0)
 
+        every = [pltpu.make_async_remote_copy(
+            src_ref=st.at[pl.ds(0, n_sp - 1)], dst_ref=gt.at[pl.ds(0, n_sp - 1)], send_sem=sends.at[n],
+            recv_sem=recvs.at[n], device_id={"sp": other(0)}, device_id_type=MESH)
+            for n, (st, gt) in enumerate(zip(stages, gots))]
+
         def collect():
-            def one(i, c):
-                frm = other(i, -1)
-                for copy in copies(i, frm, frm):
-                    copy.wait_recv()
-                return c
-            lax.fori_loop(0, n_sp - 1, one, 0)
+            for copy in every:
+                copy.wait_recv()
 
         def drain():
-            def one(i, c):
-                for copy in copies(i, other(i, 1), sp):
-                    copy.wait_send()
-                return c
-            lax.fori_loop(0, n_sp - 1, one, 0)
+            for copy in every:
+                copy.wait_send()
 
         return spread, collect, drain
 
@@ -331,19 +329,14 @@
         run = run * decay(q, 1) + got_b[q].astype(F32)
     got2[sp] = stage2[sp]
     spread2()
+    inner(early, 0)
     spread3()
-
-    lax.fori_loop(early, n_chunk, inner, 0)
-
-    def settle(j, c):
-        for kind in range(4):
-            ring(kind, j).wait_send()
-        pair(0, j, left).wait_send()
-        pair(1, j, right).wait_send()
-        pair(2, j, far).wait_send()
-        return c
-
-    lax.fori_loop(0, n_chunk, settle, 0)
+    lax.fori_loop(early + 1, n_chunk, inner, 0)
+
+    push(whole, chip(tp), left, out_sem.at[0], near_in.at[0]).wait_send()
+    push(whole, block(tp), left, out_sem.at[1], near_in.at[0]).wait_send()
+    push(whole, chip(tp), left, out_sem.at[2], near_in.at[0]).wait_send()
+    push(whole, block(tp), left, out_sem.at[3], near_in.at[0]).wait_send()
     pair_own(tp).wait_send()
     drain1()
     collect2()
@@ -412,6 +405,7 @@
                 pltpu.VMEM((tokens, depth), BF16),
                 pltpu.VMEM((5, depth, cols), BF16),
                 pltpu.VMEM((fresh, depth), BF16),
+                pltpu.VMEM((3, tokens, cols), F32),
                 pltpu.VMEM((2, cols), F32),
                 pltpu.VMEM((heads, tokens), F32),
                 pltpu.VMEM((1, cols), F32),
@@ -449,11 +443,8 @@
                 pltpu.VMEM((fresh, cols), F32),
                 pltpu.VMEM((fresh, cols), F32),
                 dma((10,)), dma((2,)),
-                dma((4, chunks)), dma((4, chunks)),
-                dma((3, chunks)), dma((3, chunks)),
-                dma((3, n_sp)), dma((3, n_sp)),
-                dma((1, n_sp)), dma((1, n_sp)),
-                dma((1, n_sp)), dma((1, n_sp)),
+                dma((4,)), dma((chunks,)), dma((chunks,)), dma((chunks,)), dma((chunks,)),
+                dma((3,)), dma((3,)), dma((1,)), dma((1,)), dma((1,)), dma((1,)),
             ],
             compiler_params=pltpu.CompilerParams(collective_id=0, has_side_effects=True,
                                                  vmem_limit_bytes=VM1 * 1024 * 1024),

time: 65.9 us -> 60.1 us (0.912)
  Pallas kernels: 65.1 us -> 59.3 us
    pallas_call x1, Pallas kernels: 64.3 us -> 58.5 us  [per_device(): pl.pallas_call(kernel, out_shape=(jax.ShapeDtypeStruct((tokens, cols), BF...]
where the time goes in v2:
time: 60.1 us; the launch traced here: 60 us
  Pallas kernels  59.3 us (99%)
  between operations  0.64 us (1%)
    pallas_call x1, Pallas kernels, per_device(): pl.pallas_call(kernel, out_shape=(jax.ShapeDtypeStruct((tokens, cols), BF...  58.5 us

profile of v2, /device:TPU:1, one launch (start us, length us, event | category | flops | bytes accessed | tf_op | source)
XLA Modules:
  0.0 60.0 jit_solution(1493009248516782956)
XLA Ops:
  0.6 58.5 %shard_map.112 = (bf16[1024,256]{1,0:T(8,128)(2,1)S(1)}, bf16[2,128,128]{2,1,0:T(8,128)(2,1)S(1)}, bf16[128,256]{1,0:T(8,128)(2,1)S(1)}) custom-call(bf16[1024,256]{1,0:T(8,128)(2,1)} %refs_0_.1, bf16[2048,256]{1,0:T(8,128)(2,1)} %refs_1_.1, bf16[2048,256]{1,0:T(8,128)(2,1)} %refs_2_.1, bf16[2,2048,256]{2,1,0:T(8,128)(2,1)} %refs_3_.1, ...), custom_call_target="tpu_custom_call" | custom-call | tf_op jit(solution)/shard_map/pallas_call | solution.py:397
  59.1 0.9 %shard_map.113 = (bf16[1024,256]{1,0:T(8,128)(2,1)}, bf16[2,128,128]{2,1,0:T(8,128)(2,1)}, bf16[128,256]{1,0:T(8,128)(2,1)}) custom-call(bf16[1024,256]{1,0:T(8,128)(2,1)S(1)} %get-tuple-element.6.a, bf16[2,128,128]{2,1,0:T(8,128)(2,1)S(1)} %get-tuple-element.7.b, bf16[128,256]{1,0:T(8,128)(2,1)S(1)} %get-tuple-element.8.c), custom_call_target="tpu_custom_call" | custom-call | tf_op jit(solution)/shard_map/pallas_call | solution.py:462

commit v3 on v2

--- a/solution.py
+++ b/solution.py
@@ -11,6 +11,7 @@
 HD = 128
 VM1 = 48
 LEAD = 3
+LAG = 2
 NX = 4
 F32 = jnp.float32
 BF16 = jnp.bfloat16
@@ -43,7 +44,7 @@
 def body(n_sp, n_tp, n_chunk, heads, x_hbm, wq, wv, wf, wg, nx_hbm, room_hbm, extra_hbm, gain_hbm,
          mixed_out, cache_out, read_out,
          x, w, nx, part, room, extra, gain, qs, vs, cf, cb, kf_s, kb_s, gs, a_f, a_b, e_f, e_b, s_f, s_b, acc,
-         inside, qc_hi, qc_lo, st_hi, st_lo, stage_f, stage_b, stage_d, got_f, got_b, got_d, stage2, got2, fin, nq_hi, nq_lo, nv, nown, ngate,
+         inside, qc, st, stage_f, stage_b, stage_d, got_f, got_b, got_d, stage2, got2, fin, nq_hi, nq_lo, nv, nown, ngate,
          load_sem, own_sem, out_sem, near_in, far_in, mate_near, mate_far, p1_send, p1_recv, p2_send, p2_recv,
          p3_send, p3_recv):
     cols = heads * HD
@@ -200,18 +201,22 @@
             c = j - 1
             push(rows(c), chip(left), mate, out_sem.at[2], mate_near.at[c]).wait_recv()
             near_part(c)
+
+        @pl.when((j >= LAG) & (j < n_chunk + LAG))
+        def _():
+            c = j - LAG
             push(rows(c), block(far), left, out_sem.at[1], far_in.at[c]).wait_recv()
             pass_far(c)
 
-        @pl.when(j >= 2)
+        @pl.when(j >= LAG + 1)
         def _():
-            c = j - 2
+            c = j - LAG - 1
             push(rows(c), block(far), mate, out_sem.at[3], mate_far.at[c]).wait_recv()
             compute(c)
 
         return carry
 
-    lax.fori_loop(0, n_chunk + 2, step, 0)
+    lax.fori_loop(0, n_chunk + LAG + 1, step, 0)
 
     per = n_sp // heads
     nz = n_sp // NX
@@ -226,12 +231,14 @@
     got_b[sp] = stage_b[sp]
     got_d[sp] = stage_d[sp]
 
-    def other(i):
-        m, n = i // NX, lax.rem(i, NX)
-        dz = nz // 2 + ((m + 1) // 2) * (1 - 2 * lax.rem(m, 2))
-        dx = NX // 2 + ((n + 1) // 2) * (1 - 2 * lax.rem(n, 2))
-        z, xx = sp // NX, lax.rem(sp, NX)
-        return lax.rem(z + dz, nz) * NX + lax.rem(xx + dx, NX)
+    my_z, my_x = sp // NX, lax.rem(sp, NX)
+
+    def outward(n):
+        return [n // 2 + ((i + 1) // 2) * (1 - 2 * (i % 2)) for i in range(n)]
+
+    z_at = {d: lax.rem(my_z + d, nz) * NX for d in range(nz)}
+    x_at = {d: lax.rem(my_x + d, NX) for d in range(NX)}
+    others = [z_at[dz] + x_at[dx] for dz in outward(nz) for dx in outward(NX) if dz or dx]
 
     def exchange(stages, gots, sends, recvs, whole=False):
         def copies(to, frm):
@@ -241,15 +248,13 @@
                 for n, (st, gt) in enumerate(zip(stages, gots))]
 
         def spread():
-            def one(i, c):
-                for copy in copies(other(i), sp):
+            for to in others:
+                for copy in copies(to, sp):
                     copy.start()
-                return c
-            lax.fori_loop(0, n_sp - 1, one, 0)
 
         every = [pltpu.make_async_remote_copy(
             src_ref=st.at[pl.ds(0, n_sp - 1)], dst_ref=gt.at[pl.ds(0, n_sp - 1)], send_sem=sends.at[n],
-            recv_sem=recvs.at[n], device_id={"sp": other(0)}, device_id_type=MESH)
+            recv_sem=recvs.at[n], device_id={"sp": others[0]}, device_id_type=MESH)
             for n, (st, gt) in enumerate(zip(stages, gots))]
 
         def collect():
@@ -290,8 +295,8 @@
             ki_b = (kb_s[r, hs] * jnp.exp(mid_b - wbh)).astype(BF16)
             sc = jnp.where(lower, nt(qi_f, ki_f), 0.0) + jnp.where(upper, nt(qi_b, ki_b), 0.0)
             inside[r, hs] = nn(sc.astype(BF16), vs[r, hs])
-            qc_hi[h, r, 0:HD], qc_lo[h, r, 0:HD] = split2(q * jnp.exp(wfh))
-            qc_hi[h, r, HD:2 * HD], qc_lo[h, r, HD:2 * HD] = split2(q * jnp.exp(wbh))
+            qc[h, c, 0:B, 0:HD], qc[h, c, B:2 * B, 0:HD] = split2(q * jnp.exp(wfh))
+            qc[h, c, 0:B, HD:2 * HD], qc[h, c, B:2 * B, HD:2 * HD] = split2(q * jnp.exp(wbh))
         return carry
 
     def inner(c, carry):
@@ -329,9 +334,8 @@
         run = run * decay(q, 1) + got_b[q].astype(F32)
     got2[sp] = stage2[sp]
     spread2()
-    inner(early, 0)
+    lax.fori_loop(early, n_chunk, inner, 0)
     spread3()
-    lax.fori_loop(early + 1, n_chunk, inner, 0)
 
     push(whole, chip(tp), left, out_sem.at[0], near_in.at[0]).wait_send()
     push(whole, block(tp), left, out_sem.at[1], near_in.at[0]).wait_send()
@@ -344,11 +348,11 @@
     for h in range(heads):
         run = got2[h * per:(h + 1) * per, 0].reshape(HD, HD)
         for c in range(n_chunk):
-            st_hi[h, c, :, 0:HD], st_lo[h, c, :, 0:HD] = split2(run)
+            st[h, c, 0:HD, 0:HD], st[h, c, HD:2 * HD, 0:HD] = split2(run)
             run = run * e_f[c, h, 0:1, :] + a_f[c, h]
         run = got2[h * per:(h + 1) * per, 1].reshape(HD, HD)
         for c in reversed(range(n_chunk)):
-            st_hi[h, c, :, HD:2 * HD], st_lo[h, c, :, HD:2 * HD] = split2(run)
+            st[h, c, 0:HD, HD:2 * HD], st[h, c, HD:2 * HD, HD:2 * HD] = split2(run)
             run = run * e_b[c, h, 0:1, :] + a_b[c, h]
 
     def norm(mix, scale):
@@ -358,12 +362,13 @@
         r = rows(c)
         for h in range(heads):
             hs = slice(h * HD, (h + 1) * HD)
-            mix = (inside[r, hs] + nt(qc_lo[h, r, :], st_hi[h, c]) + nt(qc_hi[h, r, :], st_lo[h, c])
-                   + nt(qc_hi[h, r, :], st_hi[h, c]))
+            carried = nt(qc[h, c], st[h, c])
+            carried = carried[0:B] + carried[B:2 * B]
+            mix = inside[r, hs] + (carried[:, HD:2 * HD] + carried[:, 0:HD])
             mixed_out[r, hs] = norm(mix, gs[r, hs])
         return carry
 
-    lax.fori_loop(0, n_chunk, finish, 0, unroll=2)
+    lax.fori_loop(0, n_chunk, finish, 0, unroll=8)
 
     collect3()
     for h in range(heads):
@@ -424,10 +429,8 @@
                 pltpu.VMEM((heads, HD, HD), F32),
                 pltpu.VMEM((2, heads, 8, HD), F32),
                 pltpu.VMEM((tokens, cols), F32),
-                pltpu.VMEM((heads, tokens, 2 * HD), BF16),
-                pltpu.VMEM((heads, tokens, 2 * HD), BF16),
-                pltpu.VMEM((heads, chunks, HD, 2 * HD), BF16),
-                pltpu.VMEM((heads, chunks, HD, 2 * HD), BF16),
+                pltpu.VMEM((heads, chunks, 2 * B, 2 * HD), BF16),
+                pltpu.VMEM((heads, chunks, 2 * HD, 2 * HD), BF16),
                 pltpu.VMEM((n_sp, 8, HD), F32),
                 pltpu.VMEM((n_sp, 8, HD), BF16),
                 pltpu.VMEM((n_sp, 2, HD), F32),

time: 60.1 us -> 55.4 us (0.922)
  Pallas kernels: 59.3 us -> 54.6 us
    pallas_call x1, Pallas kernels: 58.5 us -> 53.8 us  [per_device(): pl.pallas_call(kernel, out_shape=(jax.ShapeDtypeStruct((tokens, cols), BF...]
where the time goes in v3:
time: 55.4 us; the launch traced here: 55.3 us
  Pallas kernels  54.6 us (99%)
  between operations  0.64 us (1%)
    pallas_call x1, Pallas kernels, per_device(): pl.pallas_call(kernel, out_shape=(jax.ShapeDtypeStruct((tokens, cols), BF...  53.8 us

profile of v3, /device:TPU:1, one launch (start us, length us, event | category | flops | bytes accessed | tf_op | source)
XLA Modules:
  0.0 55.3 jit_solution(1057734599713724321)
XLA Ops:
  0.6 53.8 %shard_map.112 = (bf16[1024,256]{1,0:T(8,128)(2,1)S(1)}, bf16[2,128,128]{2,1,0:T(8,128)(2,1)S(1)}, bf16[128,256]{1,0:T(8,128)(2,1)S(1)}) custom-call(bf16[1024,256]{1,0:T(8,128)(2,1)} %refs_0_.1, bf16[2048,256]{1,0:T(8,128)(2,1)} %refs_1_.1, bf16[2048,256]{1,0:T(8,128)(2,1)} %refs_2_.1, bf16[2,2048,256]{2,1,0:T(8,128)(2,1)} %refs_3_.1, ...), custom_call_target="tpu_custom_call" | custom-call | tf_op jit(solution)/shard_map/pallas_call | solution.py:402
  54.4 0.9 %shard_map.113 = (bf16[1024,256]{1,0:T(8,128)(2,1)}, bf16[2,128,128]{2,1,0:T(8,128)(2,1)}, bf16[128,256]{1,0:T(8,128)(2,1)}) custom-call(bf16[1024,256]{1,0:T(8,128)(2,1)S(1)} %get-tuple-element.6.a, bf16[2,128,128]{2,1,0:T(8,128)(2,1)S(1)} %get-tuple-element.7.b, bf16[128,256]{1,0:T(8,128)(2,1)S(1)} %get-tuple-element.8.c), custom_call_target="tpu_custom_call" | custom-call | tf_op jit(solution)/shard_map/pallas_call | solution.py:465

commit v4 on v3

--- a/solution.py
+++ b/solution.py
@@ -45,7 +45,7 @@
          mixed_out, cache_out, read_out,
          x, w, nx, part, room, extra, gain, qs, vs, cf, cb, kf_s, kb_s, gs, a_f, a_b, e_f, e_b, s_f, s_b, acc,
          inside, qc, st, stage_f, stage_b, stage_d, got_f, got_b, got_d, stage2, got2, fin, nq_hi, nq_lo, nv, nown, ngate,
-         load_sem, own_sem, out_sem, near_in, far_in, mate_near, mate_far, p1_send, p1_recv, p2_send, p2_recv,
+         load_sem, own_sem, out_sem, near_in, far_in, mate_near, mate_far, word, p1_send, p1_recv, p2_send, p2_recv,
          p3_send, p3_recv):
     cols = heads * HD
     sp = lax.axis_index("sp")
@@ -56,15 +56,21 @@
     flip = 1 - 2 * lax.rem(tp, 2)
     mate = tp + flip
 
+    nz = n_sp // NX
+    my_z, my_x = sp // NX, lax.rem(sp, NX)
+
     barrier = pltpu.get_barrier_semaphore()
+    z_sides = [lax.rem(my_z + d, nz) * NX + my_x for d in (1, nz - 1)]
+    x_sides = [my_z * NX + lax.rem(my_x + d, NX) for d in (1, NX - 1)]
     for peer in (mate, left, right):
         pl.semaphore_signal(barrier, inc=1, device_id={"tp": peer}, device_id_type=MESH)
-
-    def greet(i, c):
-        pl.semaphore_signal(barrier, inc=1, device_id={"sp": lax.rem(sp + i, n_sp)}, device_id_type=MESH)
-        return c
-
-    lax.fori_loop(1, n_sp, greet, 0)
+    for peer in z_sides + x_sides:
+        pl.semaphore_signal(barrier, inc=1, device_id={"sp": peer}, device_id_type=MESH)
+    rounds = 1 + nz // 2
+
+    def tell(n, sides):
+        for peer in sides:
+            pl.semaphore_signal(word.at[n], inc=1, device_id={"sp": peer}, device_id_type=MESH)
 
     def block(owner):
         return pl.ds(pl.multiple_of(owner * cols, cols), cols)
@@ -116,9 +122,10 @@
         return push(whole, block(owner), mate, own_sem.at[0], own_sem.at[1])
 
     loads[0].wait()
-    pl.semaphore_wait(barrier, n_sp + 2)
+    pl.semaphore_wait(barrier, 7)
 
     pair_own(tp).start()
+    tell(0, x_sides)
     for j in range(LEAD):
         send_own(j)
 
@@ -196,6 +203,14 @@
         def _():
             send_own(j + LEAD)
 
+        @pl.when((j >= 1) & (j <= rounds))
+        def _():
+            pl.semaphore_wait(word.at[j - 1], 2)
+
+        @pl.when((j >= 1) & (j < rounds))
+        def _():
+            tell(j, z_sides)
+
         @pl.when((j >= 1) & (j <= n_chunk))
         def _():
             c = j - 1
@@ -219,7 +234,6 @@
     lax.fori_loop(0, n_chunk + LAG + 1, step, 0)
 
     per = n_sp // heads
-    nz = n_sp // NX
     r_id = lax.broadcasted_iota(jnp.int32, (2, HD), 0)
     for h in range(heads):
         at = slice(h * per, (h + 1) * per)
@@ -230,8 +244,6 @@
     got_f[sp] = stage_f[sp]
     got_b[sp] = stage_b[sp]
     got_d[sp] = stage_d[sp]
-
-    my_z, my_x = sp // NX, lax.rem(sp, NX)
 
     def outward(n):
         return [n // 2 + ((i + 1) // 2) * (1 - 2 * (i % 2)) for i in range(n)]
@@ -447,6 +459,7 @@
                 pltpu.VMEM((fresh, cols), F32),
                 dma((10,)), dma((2,)),
                 dma((4,)), dma((chunks,)), dma((chunks,)), dma((chunks,)), dma((chunks,)),
+                pltpu.SemaphoreType.REGULAR((1 + n_sp // NX // 2,)),
                 dma((3,)), dma((3,)), dma((1,)), dma((1,)), dma((1,)), dma((1,)),
             ],
             compiler_params=pltpu.CompilerParams(collective_id=0, has_side_effects=True,

time: 55.4 us -> 53.1 us (0.958)
  Pallas kernels: 54.6 us -> 52.4 us
    pallas_call x1, Pallas kernels: 53.8 us -> 51.5 us  [per_device(): pl.pallas_call(kernel, out_shape=(jax.ShapeDtypeStruct((tokens, cols), BF...]
where the time goes in v4:
time: 53.1 us; the launch traced here: 53 us
  Pallas kernels  52.4 us (99%)
  between operations  0.64 us (1%)
    pallas_call x1, Pallas kernels, per_device(): pl.pallas_call(kernel, out_shape=(jax.ShapeDtypeStruct((tokens, cols), BF...  51.5 us

profile of v4, /device:TPU:1, one launch (start us, length us, event | category | flops | bytes accessed | tf_op | source)
XLA Modules:
  0.0 53.0 jit_solution(4980840811669810329)
XLA Ops:
  0.6 51.5 %shard_map.112 = (bf16[1024,256]{1,0:T(8,128)(2,1)S(1)}, bf16[2,128,128]{2,1,0:T(8,128)(2,1)S(1)}, bf16[128,256]{1,0:T(8,128)(2,1)S(1)}) custom-call(bf16[1024,256]{1,0:T(8,128)(2,1)} %refs_0_.1, bf16[2048,256]{1,0:T(8,128)(2,1)} %refs_1_.1, bf16[2048,256]{1,0:T(8,128)(2,1)} %refs_2_.1, bf16[2,2048,256]{2,1,0:T(8,128)(2,1)} %refs_3_.1, ...), custom_call_target="tpu_custom_call" | custom-call | tf_op jit(solution)/shard_map/pallas_call | solution.py:414
  52.1 0.9 %shard_map.113 = (bf16[1024,256]{1,0:T(8,128)(2,1)}, bf16[2,128,128]{2,1,0:T(8,128)(2,1)}, bf16[128,256]{1,0:T(8,128)(2,1)}) custom-call(bf16[1024,256]{1,0:T(8,128)(2,1)S(1)} %get-tuple-element.6.a, bf16[2,128,128]{2,1,0:T(8,128)(2,1)S(1)} %get-tuple-element.7.b, bf16[128,256]{1,0:T(8,128)(2,1)S(1)} %get-tuple-element.8.c), custom_call_target="tpu_custom_call" | custom-call | tf_op jit(solution)/shard_map/pallas_call | solution.py:478

commit v5 on v4

--- a/solution.py
+++ b/solution.py
@@ -11,6 +11,7 @@
 HD = 128
 VM1 = 48
 LEAD = 3
+TILE = 32
 LAG = 2
 NX = 4
 F32 = jnp.float32
@@ -43,7 +44,7 @@
 
 def body(n_sp, n_tp, n_chunk, heads, x_hbm, wq, wv, wf, wg, nx_hbm, room_hbm, extra_hbm, gain_hbm,
          mixed_out, cache_out, read_out,
-         x, w, nx, part, room, extra, gain, qs, vs, cf, cb, kf_s, kb_s, gs, a_f, a_b, e_f, e_b, s_f, s_b, acc,
+         x, w, nx, part, lg, room, extra, gain, qs, vs, cf, cb, kf_s, kb_s, gs, a_f, a_b, e_f, e_b, s_f, s_b, acc,
          inside, qc, st, stage_f, stage_b, stage_d, got_f, got_b, got_d, stage2, got2, fin, nq_hi, nq_lo, nv, nown, ngate,
          load_sem, own_sem, out_sem, near_in, far_in, mate_near, mate_far, word, p1_send, p1_recv, p2_send, p2_recv,
          p3_send, p3_recv):
@@ -132,22 +133,32 @@
     kinds = (2, 3, 1)
 
     def own_part(c, carry):
-        r = rows(c)
+        r = pl.ds(pl.multiple_of(c * 2 * B, 2 * B), 2 * B)
         xc = x[r, chip(tp)]
         for n, i in enumerate(kinds):
             part[n, r, :] = nn(xc, w[i, chip(tp), :])
         return carry
 
     def near_part(c):
-        r = rows(c)
+        r = pl.ds(pl.multiple_of(c * B, B), 2 * B)
         xl, xr = x[r, chip(left)], x[r, chip(right)]
         for n, i in enumerate(kinds):
             part[n, r, :] += nn(xl, w[i, chip(left), :]) + nn(xr, w[i, chip(right), :])
 
-    for load in loads[1:6]:
+    loads[2].wait()
+    for h in range(heads):
+        ex = jnp.concatenate([extra[h:h + 1, c * B:(c + 1) * B] for c in range(n_chunk)], axis=0)
+        e_hi, e_lo = split2(ex)
+        for mask, sums in ((upper, cf), (lower, cb)):
+            tri = jnp.where(mask, 1.0, 0.0).astype(BF16)
+            down = (nn(e_hi, tri) + nn(e_lo, tri)).T
+            for c in range(n_chunk):
+                sums[c * B:(c + 1) * B, h * HD:(h + 1) * HD] = jnp.broadcast_to(down[:, c:c + 1], (B, HD))
+
+    for load in (loads[1], *loads[3:6]):
         load.wait()
     pair_own(mate).wait_recv()
-    lax.fori_loop(0, n_chunk, own_part, 0)
+    lax.fori_loop(0, n_chunk // 2, own_part, 0)
 
     s_f[...] = jnp.zeros_like(s_f)
     s_b[...] = jnp.zeros_like(s_b)
@@ -156,40 +167,36 @@
     def compute(c):
         r = rows(c)
         xc = x[r, chip(far)]
-        kf = room[0:1, :] / (1.0 + jnp.exp(part[0, r, :] + nn(xc, w[2, chip(far), :])))
-        kb = room[1:2, :] / (1.0 + jnp.exp(part[1, r, :] + nn(xc, w[3, chip(far), :])))
-        kf_s[r, :] = kf
-        kb_s[r, :] = kb
-        vc = (part[2, r, :] + nn(xc, w[1, chip(far), :])).astype(BF16)
+        far_w = chip(far)
+        part[0, r, :] += nn(xc, w[2, far_w, :])
+        part[1, r, :] += nn(xc, w[3, far_w, :])
+        vc = (part[2, r, :] + nn(xc, w[1, far_w, :])).astype(BF16)
         vs[r, :] = vc
-        tri_l = jnp.where(lower, 1.0, 0.0).astype(BF16)
-        tri_u = jnp.where(upper, 1.0, 0.0).astype(BF16)
-        lf_hi, lf_lo = split2(log_one_minus(kf))
-        lb_hi, lb_lo = split2(log_one_minus(kb))
-        wfc = nn(tri_l, lf_hi) + nn(tri_l, lf_lo)
-        wbc = nn(tri_u, lb_hi) + nn(tri_u, lb_lo)
-        ones = jnp.ones((B, HD), BF16)
+        for t in range(B // TILE):
+            rt = pl.ds(pl.multiple_of(c * B + t * TILE, TILE), TILE)
+            for d, keys in ((0, kf_s), (1, kb_s)):
+                key = room[d:d + 1, :] / (1.0 + jnp.exp(part[d, rt, :]))
+                keys[rt, :] = key
+                lg[d, t * TILE:(t + 1) * TILE], lg[d, B + t * TILE:B + (t + 1) * TILE] = split2(log_one_minus(key))
+        for d, (mask, sums) in enumerate(((lower, cf), (upper, cb))):
+            tri = jnp.where(mask, 1.0, 0.0).astype(BF16)
+            sums[r, :] += nn(jnp.concatenate([tri, tri], axis=1), lg[d])
         for h in range(heads):
             hs = slice(h * HD, (h + 1) * HD)
-            ex = extra[h:h + 1, r]
-            el_hi, el_lo = split2(jnp.where(lower, ex, 0.0))
-            eu_hi, eu_lo = split2(jnp.where(upper, ex, 0.0))
-            wfh = wfc[:, hs] + nn(el_hi, ones) + nn(el_lo, ones)
-            wbh = wbc[:, hs] + nn(eu_hi, ones) + nn(eu_lo, ones)
-            cf[r, hs] = wfh
-            cb[r, hs] = wbh
-            end_f = wfh[B - 1:B, :]
-            end_b = wbh[0:1, :]
-            ke_hi, ke_lo = split2(kf[:, hs] * jnp.exp(end_f - wfh))
-            ke_b = (kb[:, hs] * jnp.exp(end_b - wbh)).astype(BF16)
-            af = tn(vc[:, hs], ke_hi) + tn(vc[:, hs], ke_lo)
-            ab = tn(vc[:, hs], ke_b)
-            a_f[c, h] = af
-            a_b[c, h] = ab
+            wf_h, wb_h = cf[r, hs], cb[r, hs]
+            end_f, end_b = wf_h[B - 1:B, :], wb_h[0:1, :]
+            f_hi, f_lo = split2(kf_s[r, hs] * jnp.exp(end_f - wf_h))
+            b_hi, b_lo = split2(kb_s[r, hs] * jnp.exp(end_b - wb_h))
+            keys = jnp.concatenate([jnp.concatenate([f_hi, b_hi], axis=1), jnp.concatenate([f_lo, b_lo], axis=1)], axis=0)
+            vh = vc[:, hs]
+            add = tn(jnp.concatenate([vh, vh], axis=0), keys)
+            add_f, add_b = add[:, 0:HD], add[:, HD:2 * HD]
+            a_f[c, h] = add_f
+            a_b[c, h] = add_b
             e_f[c, h] = jnp.broadcast_to(jnp.exp(end_f), (8, HD))
             e_b[c, h] = jnp.broadcast_to(jnp.exp(end_b), (8, HD))
-            s_f[h] = s_f[h] * jnp.exp(end_f) + af
-            s_b[h] = s_b[h] + jnp.exp(acc[1, h, 0:1, :]) * ab
+            s_f[h] = s_f[h] * jnp.exp(end_f) + add_f
+            s_b[h] = s_b[h] + jnp.exp(acc[1, h, 0:1, :]) * add_b
             acc[0, h] = acc[0, h] + end_f
             acc[1, h] = acc[1, h] + end_b
 
@@ -215,7 +222,10 @@
         def _():
             c = j - 1
             push(rows(c), chip(left), mate, out_sem.at[2], mate_near.at[c]).wait_recv()
-            near_part(c)
+
+        @pl.when((j >= 2) & (j <= n_chunk) & (lax.rem(j, 2) == 0))
+        def _():
+            near_part(j - 2)
 
         @pl.when((j >= LAG) & (j < n_chunk + LAG))
         def _():
@@ -423,6 +433,7 @@
                 pltpu.VMEM((5, depth, cols), BF16),
                 pltpu.VMEM((fresh, depth), BF16),
                 pltpu.VMEM((3, tokens, cols), F32),
+                pltpu.VMEM((2, 2 * B, cols), BF16),
                 pltpu.VMEM((2, cols), F32),
                 pltpu.VMEM((heads, tokens), F32),
                 pltpu.VMEM((1, cols), F32),

time: 53.1 us -> 52.1 us (0.981)
  Pallas kernels: 52.4 us -> 51.4 us
    pallas_call x1, Pallas kernels: 51.5 us -> 50.6 us  [per_device(): pl.pallas_call(kernel, out_shape=(jax.ShapeDtypeStruct((tokens, cols), BF...]
where the time goes in v5:
time: 52.1 us
  Pallas kernels  51.4 us (99%)
  between operations  0.64 us (1%)
    pallas_call x1, Pallas kernels, per_device(): pl.pallas_call(kernel, out_shape=(jax.ShapeDtypeStruct((tokens, cols), BF...  50.6 us

profile of v5, /device:TPU:1, one launch (start us, length us, event | category | flops | bytes accessed | tf_op | source)
XLA Modules:
  0.0 52.1 jit_solution(17735090133328902668)
XLA Ops:
  0.6 50.6 %shard_map.112 = (bf16[1024,256]{1,0:T(8,128)(2,1)S(1)}, bf16[2,128,128]{2,1,0:T(8,128)(2,1)S(1)}, bf16[128,256]{1,0:T(8,128)(2,1)S(1)}) custom-call(bf16[1024,256]{1,0:T(8,128)(2,1)} %refs_0_.1, bf16[2048,256]{1,0:T(8,128)(2,1)} %refs_1_.1, bf16[2048,256]{1,0:T(8,128)(2,1)} %refs_2_.1, bf16[2,2048,256]{2,1,0:T(8,128)(2,1)} %refs_3_.1, ...), custom_call_target="tpu_custom_call" | custom-call | tf_op jit(solution)/shard_map/pallas_call | solution.py:424
  51.2 0.9 %shard_map.113 = (bf16[1024,256]{1,0:T(8,128)(2,1)}, bf16[2,128,128]{2,1,0:T(8,128)(2,1)}, bf16[128,256]{1,0:T(8,128)(2,1)}) custom-call(bf16[1024,256]{1,0:T(8,128)(2,1)S(1)} %get-tuple-element.6.a, bf16[2,128,128]{2,1,0:T(8,128)(2,1)S(1)} %get-tuple-element.7.b, bf16[128,256]{1,0:T(8,128)(2,1)S(1)} %get-tuple-element.8.c), custom_call_target="tpu_custom_call" | custom-call | tf_op jit(solution)/shard_map/pallas_call | solution.py:489

commit v6 on v5

--- a/solution.py
+++ b/solution.py
@@ -45,9 +45,9 @@
 def body(n_sp, n_tp, n_chunk, heads, x_hbm, wq, wv, wf, wg, nx_hbm, room_hbm, extra_hbm, gain_hbm,
          mixed_out, cache_out, read_out,
          x, w, nx, part, lg, room, extra, gain, qs, vs, cf, cb, kf_s, kb_s, gs, a_f, a_b, e_f, e_b, s_f, s_b, acc,
-         inside, qc, st, stage_f, stage_b, stage_d, got_f, got_b, got_d, stage2, got2, fin, nq_hi, nq_lo, nv, nown, ngate,
+         inside, qc, st, stage_f, stage_l, stage_b, stage_d, got_f, got_l, got_b, got_d, stage2, got2, fin, nq_hi, nq_lo, nv, nown, ngate,
          load_sem, own_sem, out_sem, near_in, far_in, mate_near, mate_far, word, p1_send, p1_recv, p2_send, p2_recv,
-         p3_send, p3_recv):
+         p3_send, p3_recv, p4_send, p4_recv):
     cols = heads * HD
     sp = lax.axis_index("sp")
     tp = lax.axis_index("tp")
@@ -247,12 +247,13 @@
     r_id = lax.broadcasted_iota(jnp.int32, (2, HD), 0)
     for h in range(heads):
         at = slice(h * per, (h + 1) * per)
-        stage_f[at] = s_f[h].reshape(per, 8, HD)
+        stage_f[at], stage_l[at] = split2(s_f[h].reshape(per, 8, HD))
         stage_b[at] = s_b[h].reshape(per, 8, HD).astype(BF16)
         both = jnp.where(r_id == 0, acc[0, h, 0:2], acc[1, h, 0:2])
         stage_d[at] = jnp.broadcast_to(both[None], (per, 2, HD))
     got_f[sp] = stage_f[sp]
     got_b[sp] = stage_b[sp]
+    got_l[sp] = stage_l[sp]
     got_d[sp] = stage_d[sp]
 
     def outward(n):
@@ -291,9 +292,11 @@
 
     spread1, collect1, drain1 = exchange((stage_d, stage_f, stage_b), (got_d, got_f, got_b), p1_send, p1_recv)
     spread2, collect2, drain2 = exchange((stage2,), (got2,), p2_send, p2_recv)
+    spread4, collect4, drain4 = exchange((stage_l,), (got_l,), p4_send, p4_recv)
     spread3, collect3, drain3 = exchange((fin,), (fin,), p3_send, p3_recv, whole=True)
 
     spread1()
+    spread4()
 
     def queries(c, carry):
         r = rows(c)
@@ -329,6 +332,31 @@
         load.wait()
     early = n_chunk // 2
     lax.fori_loop(0, early, inner, 0)
+    collect1()
+
+    def decay(q, at):
+        return jnp.exp(got_d[q, at:at + 1, :])
+
+    run = jnp.zeros((8, HD), F32)
+    before = []
+    for q in range(n_sp):
+        before.append(run)
+        run = run * decay(q, 0) + got_f[q].astype(F32)
+    run = jnp.zeros((8, HD), F32)
+    for q in reversed(range(n_sp)):
+        stage2[q, 0] = before[q]
+        stage2[q, 1] = run
+        run = run * decay(q, 1) + got_b[q].astype(F32)
+    got2[sp] = stage2[sp]
+    spread2()
+    lax.fori_loop(early, early + n_chunk // 4, inner, 0)
+    collect4()
+    run = jnp.zeros((8, HD), F32)
+    for q in range(n_sp):
+        run = run * decay(q, 0) + (got_f[q].astype(F32) + got_l[q].astype(F32))
+    fin[sp] = run.astype(BF16)
+    spread3()
+    lax.fori_loop(early + n_chunk // 4, n_chunk, inner, 0)
     new = nx[...]
     nqf = nn(new, w[0]).astype(BF16).astype(F32)
     nv[...] = nn(new, w[1]).astype(BF16)
@@ -338,26 +366,6 @@
     nq_hi[...], nq_lo[...] = split2(nqf * (1.0 - nf))
     nown[...] = nqf * (nf + nb)
 
-    collect1()
-
-    def decay(q, at):
-        return jnp.exp(got_d[q, at:at + 1, :])
-
-    run = jnp.zeros((8, HD), F32)
-    before = []
-    for q in range(n_sp):
-        before.append(run)
-        run = run * decay(q, 0) + got_f[q]
-    fin[sp] = run.astype(BF16)
-    run = jnp.zeros((8, HD), F32)
-    for q in reversed(range(n_sp)):
-        stage2[q, 0] = before[q]
-        stage2[q, 1] = run
-        run = run * decay(q, 1) + got_b[q].astype(F32)
-    got2[sp] = stage2[sp]
-    spread2()
-    lax.fori_loop(early, n_chunk, inner, 0)
-    spread3()
 
     push(whole, chip(tp), left, out_sem.at[0], near_in.at[0]).wait_send()
     push(whole, block(tp), left, out_sem.at[1], near_in.at[0]).wait_send()
@@ -365,6 +373,7 @@
     push(whole, block(tp), left, out_sem.at[3], near_in.at[0]).wait_send()
     pair_own(tp).wait_send()
     drain1()
+    drain4()
     collect2()
 
     for h in range(heads):
@@ -454,10 +463,12 @@
                 pltpu.VMEM((tokens, cols), F32),
                 pltpu.VMEM((heads, chunks, 2 * B, 2 * HD), BF16),
                 pltpu.VMEM((heads, chunks, 2 * HD, 2 * HD), BF16),
-                pltpu.VMEM((n_sp, 8, HD), F32),
+                pltpu.VMEM((n_sp, 8, HD), BF16),
+                pltpu.VMEM((n_sp, 8, HD), BF16),
                 pltpu.VMEM((n_sp, 8, HD), BF16),
                 pltpu.VMEM((n_sp, 2, HD), F32),
-                pltpu.VMEM((n_sp, 8, HD), F32),
+                pltpu.VMEM((n_sp, 8, HD), BF16),
+                pltpu.VMEM((n_sp, 8, HD), BF16),
                 pltpu.VMEM((n_sp, 8, HD), BF16),
                 pltpu.VMEM((n_sp, 2, HD), F32),
                 pltpu.VMEM((n_sp, 2, 8, HD), F32),
@@ -471,7 +482,7 @@
                 dma((10,)), dma((2,)),
                 dma((4,)), dma((chunks,)), dma((chunks,)), dma((chunks,)), dma((chunks,)),
                 pltpu.SemaphoreType.REGULAR((1 + n_sp // NX // 2,)),
-                dma((3,)), dma((3,)), dma((1,)), dma((1,)), dma((1,)), dma((1,)),
+                dma((3,)), dma((3,)), dma((1,)), dma((1,)), dma((1,)), dma((1,)), dma((1,)), dma((1,)),
             ],
             compiler_params=pltpu.CompilerParams(collective_id=0, has_side_effects=True,
                                                  vmem_limit_bytes=VM1 * 1024 * 1024),

time: 52.1 us -> 50.2 us (0.964)
  Pallas kernels: 51.4 us -> 49.2 us
    pallas_call x1, Pallas kernels: 50.6 us -> 48.4 us  [per_device(): pl.pallas_call(kernel, out_shape=(jax.ShapeDtypeStruct((tokens, cols), BF...]
where the time goes in v6:
time: 50.2 us; the launch traced here: 49.9 us
  Pallas kernels  49.2 us (98%)
  between operations  0.64 us (1%)
    pallas_call x1, Pallas kernels, per_device(): pl.pallas_call(kernel, out_shape=(jax.ShapeDtypeStruct((tokens, cols), BF...  48.4 us

profile of v6, /device:TPU:1, one launch (start us, length us, event | category | flops | bytes accessed | tf_op | source)
XLA Modules:
  0.0 49.9 jit_solution(16389689928446091270)
XLA Ops:
  0.6 48.4 %shard_map.112 = (bf16[1024,256]{1,0:T(8,128)(2,1)S(1)}, bf16[2,128,128]{2,1,0:T(8,128)(2,1)S(1)}, bf16[128,256]{1,0:T(8,128)(2,1)S(1)}) custom-call(bf16[1024,256]{1,0:T(8,128)(2,1)} %refs_0_.1, bf16[2048,256]{1,0:T(8,128)(2,1)} %refs_1_.1, bf16[2048,256]{1,0:T(8,128)(2,1)} %refs_2_.1, bf16[2,2048,256]{2,1,0:T(8,128)(2,1)} %refs_3_.1, ...), custom_call_target="tpu_custom_call" | custom-call | tf_op jit(solution)/shard_map/pallas_call | solution.py:433
  49.0 0.9 %shard_map.113 = (bf16[1024,256]{1,0:T(8,128)(2,1)}, bf16[2,128,128]{2,1,0:T(8,128)(2,1)}, bf16[128,256]{1,0:T(8,128)(2,1)}) custom-call(bf16[1024,256]{1,0:T(8,128)(2,1)S(1)} %get-tuple-element.6.a, bf16[2,128,128]{2,1,0:T(8,128)(2,1)S(1)} %get-tuple-element.7.b, bf16[128,256]{1,0:T(8,128)(2,1)S(1)} %get-tuple-element.8.c), custom_call_target="tpu_custom_call" | custom-call | tf_op jit(solution)/shard_map/pallas_call | solution.py:500

commit v7 on v6

--- a/solution.py
+++ b/solution.py
@@ -45,9 +45,10 @@
 def body(n_sp, n_tp, n_chunk, heads, x_hbm, wq, wv, wf, wg, nx_hbm, room_hbm, extra_hbm, gain_hbm,
          mixed_out, cache_out, read_out,
          x, w, nx, part, lg, room, extra, gain, qs, vs, cf, cb, kf_s, kb_s, gs, a_f, a_b, e_f, e_b, s_f, s_b, acc,
-         inside, qc, st, stage_f, stage_l, stage_b, stage_d, got_f, got_l, got_b, got_d, stage2, got2, fin, nq_hi, nq_lo, nv, nown, ngate,
+         inside, qc, st, stage_f, stage_l, stage_b, stage_d, got_f, got_l, got_b, got_d, out_f, out_b, in_f, in_b, fin, nq_hi, nq_lo, nv, nown, ngate,
          load_sem, own_sem, out_sem, near_in, far_in, mate_near, mate_far, word, p1_send, p1_recv, p2_send, p2_recv,
-         p3_send, p3_recv, p4_send, p4_recv):
+         p3_send, p3_recv, p4_send, p4_recv,
+         p5_send, p5_recv, p6_send, p6_recv):
     cols = heads * HD
     sp = lax.axis_index("sp")
     tp = lax.axis_index("tp")
@@ -60,6 +61,11 @@
     nz = n_sp // NX
     my_z, my_x = sp // NX, lax.rem(sp, NX)
 
+    def block(owner):
+        return pl.ds(pl.multiple_of(owner * cols, cols), cols)
+
+    own_load = pltpu.make_async_copy(x_hbm, x.at[:, block(tp)], load_sem.at[0])
+    own_load.start()
     barrier = pltpu.get_barrier_semaphore()
     z_sides = [lax.rem(my_z + d, nz) * NX + my_x for d in (1, nz - 1)]
     x_sides = [my_z * NX + lax.rem(my_x + d, NX) for d in (1, NX - 1)]
@@ -73,14 +79,11 @@
         for peer in sides:
             pl.semaphore_signal(word.at[n], inc=1, device_id={"sp": peer}, device_id_type=MESH)
 
-    def block(owner):
-        return pl.ds(pl.multiple_of(owner * cols, cols), cols)
-
     def rows(j):
         return pl.ds(pl.multiple_of(j * B, B), B)
 
-    loads = [pltpu.make_async_copy(src, dst, load_sem.at[i]) for i, (src, dst) in enumerate((
-        (x_hbm, x.at[:, block(tp)]), (room_hbm, room), (extra_hbm, extra), (wf.at[0], w.at[2]), (wf.at[1], w.at[3]),
+    loads = [pltpu.make_async_copy(src, dst, load_sem.at[i + 1]) for i, (src, dst) in enumerate((
+        (room_hbm, room), (extra_hbm, extra), (wf.at[0], w.at[2]), (wf.at[1], w.at[3]),
         (wv, w.at[1]), (gain_hbm, gain), (wq, w.at[0]), (wg, w.at[4]), (nx_hbm, nx)))]
     for load in loads:
         load.start()
@@ -122,7 +125,7 @@
     def pair_own(owner):
         return push(whole, block(owner), mate, own_sem.at[0], own_sem.at[1])
 
-    loads[0].wait()
+    own_load.wait()
     pl.semaphore_wait(barrier, 7)
 
     pair_own(tp).start()
@@ -145,7 +148,7 @@
         for n, i in enumerate(kinds):
             part[n, r, :] += nn(xl, w[i, chip(left), :]) + nn(xr, w[i, chip(right), :])
 
-    loads[2].wait()
+    loads[1].wait()
     for h in range(heads):
         ex = jnp.concatenate([extra[h:h + 1, c * B:(c + 1) * B] for c in range(n_chunk)], axis=0)
         e_hi, e_lo = split2(ex)
@@ -155,7 +158,7 @@
             for c in range(n_chunk):
                 sums[c * B:(c + 1) * B, h * HD:(h + 1) * HD] = jnp.broadcast_to(down[:, c:c + 1], (B, HD))
 
-    for load in (loads[1], *loads[3:6]):
+    for load in (loads[0], *loads[2:5]):
         load.wait()
     pair_own(mate).wait_recv()
     lax.fori_loop(0, n_chunk // 2, own_part, 0)
@@ -290,12 +293,15 @@
 
         return spread, collect, drain
 
-    spread1, collect1, drain1 = exchange((stage_d, stage_f, stage_b), (got_d, got_f, got_b), p1_send, p1_recv)
-    spread2, collect2, drain2 = exchange((stage2,), (got2,), p2_send, p2_recv)
+    spread1, collect1, drain1 = exchange((stage_d, stage_f), (got_d, got_f), p1_send, p1_recv)
+    spread5, collect5, drain5 = exchange((stage_b,), (got_b,), p5_send, p5_recv)
+    spread2, collect2, drain2 = exchange((out_f,), (in_f,), p2_send, p2_recv)
+    spread6, collect6, drain6 = exchange((out_b,), (in_b,), p6_send, p6_recv)
     spread4, collect4, drain4 = exchange((stage_l,), (got_l,), p4_send, p4_recv)
     spread3, collect3, drain3 = exchange((fin,), (fin,), p3_send, p3_recv, whole=True)
 
     spread1()
+    spread5()
     spread4()
 
     def queries(c, carry):
@@ -328,7 +334,7 @@
         queries(c, 0)
         return scores(c, 0)
 
-    for load in loads[6:]:
+    for load in loads[5:]:
         load.wait()
     early = n_chunk // 2
     lax.fori_loop(0, early, inner, 0)
@@ -338,17 +344,18 @@
         return jnp.exp(got_d[q, at:at + 1, :])
 
     run = jnp.zeros((8, HD), F32)
-    before = []
     for q in range(n_sp):
-        before.append(run)
+        out_f[q] = run
         run = run * decay(q, 0) + got_f[q].astype(F32)
+    in_f[sp] = out_f[sp]
+    spread2()
+    collect5()
     run = jnp.zeros((8, HD), F32)
     for q in reversed(range(n_sp)):
-        stage2[q, 0] = before[q]
-        stage2[q, 1] = run
+        out_b[q] = run
         run = run * decay(q, 1) + got_b[q].astype(F32)
-    got2[sp] = stage2[sp]
-    spread2()
+    in_b[sp] = out_b[sp]
+    spread6()
     lax.fori_loop(early, early + n_chunk // 4, inner, 0)
     collect4()
     run = jnp.zeros((8, HD), F32)
@@ -373,15 +380,17 @@
     push(whole, block(tp), left, out_sem.at[3], near_in.at[0]).wait_send()
     pair_own(tp).wait_send()
     drain1()
+    drain5()
     drain4()
     collect2()
+    collect6()
 
     for h in range(heads):
-        run = got2[h * per:(h + 1) * per, 0].reshape(HD, HD)
+        run = in_f[h * per:(h + 1) * per].reshape(HD, HD)
         for c in range(n_chunk):
             st[h, c, 0:HD, 0:HD], st[h, c, HD:2 * HD, 0:HD] = split2(run)
             run = run * e_f[c, h, 0:1, :] + a_f[c, h]
-        run = got2[h * per:(h + 1) * per, 1].reshape(HD, HD)
+        run = in_b[h * per:(h + 1) * per].reshape(HD, HD)
         for c in reversed(range(n_chunk)):
             st[h, c, 0:HD, HD:2 * HD], st[h, c, HD:2 * HD, HD:2 * HD] = split2(run)
             run = run * e_b[c, h, 0:1, :] + a_b[c, h]
@@ -411,6 +420,7 @@
         read_out[:, hs] = norm(nt(nq_lo[:, hs], cached) + nt(nq_hi[:, hs], cached) + own, ngate[:, hs])
 
     drain2()
+    drain6()
     drain3()
 
 
@@ -471,8 +481,10 @@
                 pltpu.VMEM((n_sp, 8, HD), BF16),
                 pltpu.VMEM((n_sp, 8, HD), BF16),
                 pltpu.VMEM((n_sp, 2, HD), F32),
-                pltpu.VMEM((n_sp, 2, 8, HD), F32),
-                pltpu.VMEM((n_sp, 2, 8, HD), F32),
+                pltpu.VMEM((n_sp, 8, HD), F32),
+                pltpu.VMEM((n_sp, 8, HD), F32),
+                pltpu.VMEM((n_sp, 8, HD), F32),
+                pltpu.VMEM((n_sp, 8, HD), F32),
                 pltpu.VMEM((n_sp, 8, HD), BF16),
                 pltpu.VMEM((fresh, cols), BF16),
                 pltpu.VMEM((fresh, cols), BF16),
@@ -482,7 +494,8 @@
                 dma((10,)), dma((2,)),
                 dma((4,)), dma((chunks,)), dma((chunks,)), dma((chunks,)), dma((chunks,)),
                 pltpu.SemaphoreType.REGULAR((1 + n_sp // NX // 2,)),
-                dma((3,)), dma((3,)), dma((1,)), dma((1,)), dma((1,)), dma((1,)), dma((1,)), dma((1,)),
+                dma((2,)), dma((2,)), dma((1,)), dma((1,)), dma((1,)), dma((1,)), dma((1,)), dma((1,)),
+                dma((1,)), dma((1,)), dma((1,)), dma((1,)),
             ],
             compiler_params=pltpu.CompilerParams(collective_id=0, has_side_effects=True,
                                                  vmem_limit_bytes=VM1 * 1024 * 1024),

time: 50.2 us -> 49.9 us (level)
  no operation moved by 1% of the time
where the time goes in v7:
time: 49.9 us
  Pallas kernels  49.2 us (99%)
  between operations  0.64 us (1%)
    pallas_call x1, Pallas kernels, per_device(): pl.pallas_call(kernel, out_shape=(jax.ShapeDtypeStruct((tokens, cols), BF...  48.4 us

profile of v7, /device:TPU:1, one launch (start us, length us, event | category | flops | bytes accessed | tf_op | source)
XLA Modules:
  0.0 49.9 jit_solution(472717005252391678)
XLA Ops:
  0.6 48.4 %shard_map.112 = (bf16[1024,256]{1,0:T(8,128)(2,1)S(1)}, bf16[2,128,128]{2,1,0:T(8,128)(2,1)S(1)}, bf16[128,256]{1,0:T(8,128)(2,1)S(1)}) custom-call(bf16[1024,256]{1,0:T(8,128)(2,1)} %refs_0_.1, bf16[2048,256]{1,0:T(8,128)(2,1)} %refs_1_.1, bf16[2048,256]{1,0:T(8,128)(2,1)} %refs_2_.1, bf16[2,2048,256]{2,1,0:T(8,128)(2,1)} %refs_3_.1, ...), custom_call_target="tpu_custom_call" | custom-call | tf_op jit(solution)/shard_map/pallas_call | solution.py:443
  49.0 0.9 %shard_map.113 = (bf16[1024,256]{1,0:T(8,128)(2,1)}, bf16[2,128,128]{2,1,0:T(8,128)(2,1)}, bf16[128,256]{1,0:T(8,128)(2,1)}) custom-call(bf16[1024,256]{1,0:T(8,128)(2,1)S(1)} %get-tuple-element.6.a, bf16[2,128,128]{2,1,0:T(8,128)(2,1)S(1)} %get-tuple-element.7.b, bf16[128,256]{1,0:T(8,128)(2,1)S(1)} %get-tuple-element.8.c), custom_call_target="tpu_custom_call" | custom-call | tf_op jit(solution)/shard_map/pallas_call | solution.py:513

commit v8 on v7

--- a/solution.py
+++ b/solution.py
@@ -356,14 +356,14 @@
         run = run * decay(q, 1) + got_b[q].astype(F32)
     in_b[sp] = out_b[sp]
     spread6()
-    lax.fori_loop(early, early + n_chunk // 4, inner, 0)
+    inner(early, 0)
     collect4()
     run = jnp.zeros((8, HD), F32)
     for q in range(n_sp):
         run = run * decay(q, 0) + (got_f[q].astype(F32) + got_l[q].astype(F32))
     fin[sp] = run.astype(BF16)
     spread3()
-    lax.fori_loop(early + n_chunk // 4, n_chunk, inner, 0)
+    lax.fori_loop(early + 1, n_chunk, inner, 0)
     new = nx[...]
     nqf = nn(new, w[0]).astype(BF16).astype(F32)
     nv[...] = nn(new, w[1]).astype(BF16)
@@ -383,13 +383,14 @@
     drain5()
     drain4()
     collect2()
-    collect6()
 
     for h in range(heads):
         run = in_f[h * per:(h + 1) * per].reshape(HD, HD)
         for c in range(n_chunk):
             st[h, c, 0:HD, 0:HD], st[h, c, HD:2 * HD, 0:HD] = split2(run)
             run = run * e_f[c, h, 0:1, :] + a_f[c, h]
+    collect6()
+    for h in range(heads):
         run = in_b[h * per:(h + 1) * per].reshape(HD, HD)
         for c in reversed(range(n_chunk)):
             st[h, c, 0:HD, HD:2 * HD], st[h, c, HD:2 * HD, HD:2 * HD] = split2(run)

time: 49.9 us -> 49.9 us (level)
  no operation moved by 1% of the time
where the time goes in v8:
time: 49.9 us; the launch traced here: 49.8 us
  Pallas kernels  49.2 us (99%)
  between operations  0.64 us (1%)
    pallas_call x1, Pallas kernels, per_device(): pl.pallas_call(kernel, out_shape=(jax.ShapeDtypeStruct((tokens, cols), BF...  48.3 us

profile of v8, /device:TPU:1, one launch (start us, length us, event | category | flops | bytes accessed | tf_op | source)
XLA Modules:
  0.0 49.8 jit_solution(14170706061333412216)
XLA Ops:
  0.6 48.3 %shard_map.112 = (bf16[1024,256]{1,0:T(8,128)(2,1)S(1)}, bf16[2,128,128]{2,1,0:T(8,128)(2,1)S(1)}, bf16[128,256]{1,0:T(8,128)(2,1)S(1)}) custom-call(bf16[1024,256]{1,0:T(8,128)(2,1)} %refs_0_.1, bf16[2048,256]{1,0:T(8,128)(2,1)} %refs_1_.1, bf16[2048,256]{1,0:T(8,128)(2,1)} %refs_2_.1, bf16[2,2048,256]{2,1,0:T(8,128)(2,1)} %refs_3_.1, ...), custom_call_target="tpu_custom_call" | custom-call | tf_op jit(solution)/shard_map/pallas_call | solution.py:444
  49.0 0.9 %shard_map.113 = (bf16[1024,256]{1,0:T(8,128)(2,1)}, bf16[2,128,128]{2,1,0:T(8,128)(2,1)}, bf16[128,256]{1,0:T(8,128)(2,1)}) custom-call(bf16[1024,256]{1,0:T(8,128)(2,1)S(1)} %get-tuple-element.6.a, bf16[2,128,128]{2,1,0:T(8,128)(2,1)S(1)} %get-tuple-element.7.b, bf16[128,256]{1,0:T(8,128)(2,1)S(1)} %get-tuple-element.8.c), custom_call_target="tpu_custom_call" | custom-call | tf_op jit(solution)/shard_map/pallas_call | solution.py:514
